TPU v7x, 32 devices: a whole 2x2x4 slice. The times are simulated.
32 devices in a mesh: ra: 8 (over z, x), cb: 4 (over y, core).
Axes of the slice: x: 2, y: 2, z: 4, core: 2. Of those that a mesh axis runs over, the one named last changes fastest.
Arguments:
- inputs: bfloat16 [1536, 4096], P(None, 'ra'), may hold values from -12 to 12
- gate_weight: bfloat16 [2, 4096, 11264], P(None, 'ra', 'cb'), may hold values from -0.09375 to 0.09375
- up_weight: bfloat16 [2, 4096, 11264], P(None, 'ra', 'cb'), may hold values from -0.09375 to 0.09375
- down_weight: bfloat16 [2, 11264, 4096], P(None, 'cb', 'ra'), may hold values from -0.0546875 to 0.0546875
- norm_gain: float32 [2, 4096], P(None, 'ra'), may hold values from 0.05 to 8
- norm_shift: float32 [2, 4096], P(None, 'ra'), may hold values from -1.5 to 1.5
Outputs:
- outputs: bfloat16 [1536, 4096], P(None, 'ra')
All inputs are finite; a program needn't handle non-finite values.
Results may differ from a plain program's by a relative error of at most 0.04.
Values may be sent and summed in bfloat16 or wider, within the bound.
A program may use at most 128 MiB of HBM per device.

v0:
```python
import jax
import jax.numpy as jnp
from jax import lax
from jax.sharding import PartitionSpec as P

LAYERS = 2


RESIDUAL = 0.5
EPSILON = 1e-05


def scale_rows(mixed_rows, row_sum, row_squares, gain_row, shift_row, full_width):
    mean_rows = row_sum / full_width
    var_rows = row_squares / full_width - mean_rows * mean_rows
    normed = (mixed_rows - mean_rows[:, None]) * lax.rsqrt(var_rows + EPSILON)[:, None]
    return (normed * gain_row + shift_row).astype(jnp.bfloat16)


def sublayer(stream, w_gate, w_up, w_down, gain_row, shift_row):
    columns = w_gate.shape[1]
    paired = jnp.concatenate((w_gate, w_up), axis=1)
    full_width = stream.shape[1] * lax.axis_size("ra")
    summed = lax.psum_scatter(
        jnp.dot(stream, paired, preferred_element_type=jnp.float32).astype(jnp.bfloat16),
        "ra",
        scatter_dimension=0,
        tiled=True,
    ).astype(jnp.float32)
    hidden = (jax.nn.silu(summed[:, :columns]) * summed[:, columns:]).astype(jnp.bfloat16)
    partial_value = jnp.dot(
        lax.all_gather(hidden, "ra", axis=0, tiled=True), w_down, preferred_element_type=jnp.float32
    )
    branch = lax.psum_scatter(
        partial_value.astype(jnp.bfloat16), "cb", scatter_dimension=0, tiled=True
    ).astype(jnp.float32)
    row_count = branch.shape[0]
    own_rows = lax.dynamic_slice_in_dim(stream, lax.axis_index("cb") * row_count, row_count, 0)
    mixed_rows = RESIDUAL * own_rows.astype(jnp.float32) + branch
    row_sum, row_squares = lax.psum(
        (jnp.sum(mixed_rows, axis=1), jnp.sum(mixed_rows * mixed_rows, axis=1)), "ra"
    )
    normed = scale_rows(mixed_rows, row_sum, row_squares, gain_row, shift_row, full_width)
    return lax.all_gather(normed, "cb", axis=0, tiled=True)


def per_device(inputs, gate_weight, up_weight, down_weight, norm_gain, norm_shift):
    stream = inputs
    for layer_index in range(LAYERS):
        stream = sublayer(
            stream,
            gate_weight[layer_index],
            up_weight[layer_index],
            down_weight[layer_index],
            norm_gain[layer_index],
            norm_shift[layer_index],
        )
    return stream


def solution(mesh):
    return jax.shard_map(
        per_device,
        mesh=mesh,
        in_specs=(
            P(None, "ra"),
            P(None, "ra", "cb"),
            P(None, "ra", "cb"),
            P(None, "cb", "ra"),
            P(None, "ra"),
            P(None, "ra"),
        ),
        out_specs=P(None, "ra"),
        check_vma=False,
    )
```

profile of v0, /device:TPU:0, one launch (start us, length us, event | category | flops | bytes accessed | tf_op | source)
XLA Modules:
  0.0 1071.8 jit_solution(15673119696770834932)
XLA Ops:
  6.5 0.0 copy-start.1
  6.5 0.0 reduce-scatter.13.cloned.1.call-start
  6.5 8.0 slice_bitcast_fusion
  14.6 0.0 copy-done.1
  14.6 14.3 %fusion = bf16[1536,5632]{0,1:T(8,128)(2,1)} fusion(bf16[1536,512]{1,0:T(8,128)(2,1)S(1)} %copy-done.1, bf16[512,2816]{1,0:T(8,128)(2,1)S(1)} %get-tuple-element.16, bf16[512,2816]{1,0:T(8,128)(2,1)} %get-tuple-element.25), kind=kOutput, calls=%fused_computation.2 | convolution fusion | flops 8878555136 | bytes 24641536 | tf_op jit(solution)/shard_map/dot_general | solution.py:25
  28.8 21.4 %copy.11 = bf16[1536,5632]{1,0:T(8,128)(2,1)} copy(bf16[1536,5632]{0,1:T(8,128)(2,1)} %fusion) | data formatting | bytes 34603008
  50.3 0.0 reduce-scatter.13.cloned.1.call-update
  50.3 0.0 all-gather.5.cloned.1.call-start
  50.3 290.0 %reduce-scatter.13.cloned.1.call-done = bf16[192,5632]{1,0:T(8,128)(2,1)} async-done(((bf16[1536,5632]{1,0:T(8,128)(2,1)}), bf16[192,5632]{1,0:T(8,128)(2,1)}) %reduce-scatter.13.cloned.1.call-update) | async-done | bytes 2162704
  340.3 3.0 copy.12
  343.3 0.5 convert_element_type.48
  343.7 0.8 fusion.8
  344.6 1.4 copy.8
  346.0 0.0 all-gather.5.cloned.1.call-update
  346.0 0.0 copy-start.3
  346.1 0.0 copy-start.4
  346.1 0.0 reduce-scatter.9.cloned.1.call-start
  346.1 126.8 %all-gather.5.cloned.1.call-done = bf16[1536,2816]{1,0:T(8,128)(2,1)} async-done(((bf16[192,2816]{1,0:T(8,128)(2,1)}), bf16[1536,2816]{1,0:T(8,128)(2,1)}) %all-gather.5.cloned.1.call-update) | async-done | bytes 8650768 | tf_op jit(solution)/shard_map/all_gather | solution.py:32
  473.0 10.1 convolution_convert_fusion.3
  483.0 0.0 copy-start
  483.0 0.0 reduce-scatter.9.cloned.1.call-update
  483.1 0.0 all-gather.7.cloned.1.call-start
  483.1 0.0 copy-done.3
  483.1 0.0 copy-done.4
  483.2 26.3 %reduce-scatter.9.cloned.1.call-done = bf16[384,512]{1,0:T(8,128)(2,1)} async-done(((bf16[1536,512]{1,0:T(8,128)(2,1)}), bf16[384,512]{1,0:T(8,128)(2,1)}) %reduce-scatter.9.cloned.1.call-update) | async-done | bytes 393232 | tf_op jit(solution)/shard_map/reduce_scatter | solution.py:34
  509.5 1.4 fusion.13
  510.8 21.4 %all-reduce.1 = (f32[384]{0:T(512)S(1)}, f32[384]{0:T(512)S(1)}) all-reduce(f32[384]{0:T(512)S(1)} %get-tuple-element.8, f32[384]{0:T(512)S(1)} %get-tuple-element.7), channel_id=1, replica_groups=mesh['ra'=8,'cb'=4] {'ra'}, use_global_device_ids=true, to_apply=%region_5.6 | all-reduce | flops 768 | bytes 6144 | tf_op jit(solution)/shard_map/psum | solution.py:40
  532.2 2.1 add_convert_fusion.1
  534.3 0.0 all-gather.7.cloned.1.call-update
  534.3 0.2 reduce-scatter.15.cloned.1.call-start
  534.6 15.9 %all-gather.7.cloned.1.call-done = bf16[1536,512]{1,0:T(8,128)(2,1)} async-done(((bf16[384,512]{1,0:T(8,128)(2,1)}), bf16[1536,512]{1,0:T(8,128)(2,1)}) %all-gather.7.cloned.1.call-update) | async-done | bytes 1572880 | tf_op jit(solution)/shard_map/all_gather | solution.py:44
  550.4 0.0 copy-done
  550.4 14.7 %convolution_convert_fusion = bf16[1536,5632]{1,0:T(8,128)(2,1)} fusion(bf16[1536,512]{1,0:T(8,128)(2,1)} %all-gather.7.cloned.1.call-done, bf16[512,2816]{1,0:T(8,128)(2,1)S(1)} %copy-done, bf16[512,2816]{1,0:T(8,128)(2,1)} %get-tuple-element.26), kind=kOutput, calls=%fused_computation | convolution fusion | flops 8878555136 | bytes 24641536 | tf_op jit(solution)/shard_map/dot_general | solution.py:25
  565.1 0.0 reduce-scatter.15.cloned.1.call-update
  565.2 0.0 all-gather.9.cloned.1.call-start
  565.2 287.2 %reduce-scatter.15.cloned.1.call-done = bf16[192,5632]{1,0:T(8,128)(2,1)} async-done(((bf16[1536,5632]{1,0:T(8,128)(2,1)}), bf16[192,5632]{1,0:T(8,128)(2,1)}) %reduce-scatter.15.cloned.1.call-update) | async-done | bytes 2162704
  852.4 3.0 copy.14
  855.4 0.5 convert_element_type.55
  855.9 0.8 fusion.7
  856.7 1.4 copy.10
  858.2 0.0 all-gather.9.cloned.1.call-update
  858.2 0.0 copy-start.2
  858.2 0.0 reduce-scatter.11.cloned.1.call-start
  858.3 126.8 %all-gather.9.cloned.1.call-done = bf16[1536,2816]{1,0:T(8,128)(2,1)} async-done(((bf16[192,2816]{1,0:T(8,128)(2,1)}), bf16[1536,2816]{1,0:T(8,128)(2,1)}) %all-gather.9.cloned.1.call-update) | async-done | bytes 8650768 | tf_op jit(solution)/shard_map/all_gather | solution.py:32
  985.1 10.1 convolution_convert_fusion.2
  995.2 0.0 reduce-scatter.11.cloned.1.call-update
  995.2 0.0 all-gather.11.cloned.1.call-start
  995.2 26.4 %reduce-scatter.11.cloned.1.call-done = bf16[384,512]{1,0:T(8,128)(2,1)} async-done(((bf16[1536,512]{1,0:T(8,128)(2,1)}), bf16[384,512]{1,0:T(8,128)(2,1)}) %reduce-scatter.11.cloned.1.call-update) | async-done | bytes 393232 | tf_op jit(solution)/shard_map/reduce_scatter | solution.py:34
  1021.6 0.0 copy-done.2
  1021.6 1.3 fusion.14
  1022.9 21.4 %all-reduce = (f32[384]{0:T(512)S(1)}, f32[384]{0:T(512)S(1)}) all-reduce(f32[384]{0:T(512)S(1)} %get-tuple-element.6, f32[384]{0:T(512)S(1)} %get-tuple-element.5), channel_id=1, replica_groups=mesh['ra'=8,'cb'=4] {'ra'}, use_global_device_ids=true, to_apply=%region_11.12 | all-reduce | flops 768 | bytes 6144 | tf_op jit(solution)/shard_map/psum | solution.py:40
  1044.2 2.0 add_convert_fusion
  1046.2 0.0 all-gather.11.cloned.1.call-update
  1046.2 16.1 %all-gather.11.cloned.1.call-done = bf16[1536,512]{1,0:T(8,128)(2,1)} async-done(((bf16[384,512]{1,0:T(8,128)(2,1)}), bf16[1536,512]{1,0:T(8,128)(2,1)}) %all-gather.11.cloned.1.call-update) | async-done | bytes 1572880 | tf_op jit(solution)/shard_map/all_gather | solution.py:44
  1062.3 2.7 copy.16
  (4 shorter events, 0.0 us)
Async XLA Ops:
  6.5 8.0 copy-start.1
  6.5 333.8 %reduce-scatter.13.cloned.1.call-start = ((), (), s32[]{:S(2)}) async-start(), calls=%async_computation.10 | async-start | bytes 19464192
  50.3 422.7 %all-gather.5.cloned.1.call-start = ((), (), s32[]{:S(2)}) async-start(), calls=%async_computation.4 | async-start | bytes 9732096 | tf_op jit(solution)/shard_map/all_gather | solution.py:32
  346.0 137.1 %copy-start.3 = (f32[2,512]{1,0:T(2,128)S(1)}, f32[2,512]{1,0:T(2,128)}, u32[]{:S(2)}) copy-start(f32[2,512]{1,0:T(2,128)} %param.11) | copy-start | bytes 12292
  346.1 137.1 %copy-start.4 = (f32[2,512]{1,0:T(2,128)S(1)}, f32[2,512]{1,0:T(2,128)}, u32[]{:S(2)}) copy-start(f32[2,512]{1,0:T(2,128)} %param.10) | copy-start | bytes 12292
  346.1 163.4 %reduce-scatter.9.cloned.1.call-start = ((), (), s32[]{:S(2)}) async-start(), calls=%async_computation.5 | async-start | bytes 1966080 | tf_op jit(solution)/shard_map/reduce_scatter | solution.py:34
  483.0 67.4 %copy-start = (bf16[512,2816]{1,0:T(8,128)(2,1)S(1)}, bf16[512,2816]{1,0:T(8,128)(2,1)}, u32[]{:S(2)}) copy-start(bf16[512,2816]{1,0:T(8,128)(2,1)} %get-tuple-element.15) | copy-start | bytes 8650756
  483.1 67.4 %all-gather.7.cloned.1.call-start = ((), (), s32[]{:S(2)}) async-start(), calls=%async_computation.6 | async-start | bytes 1966080 | tf_op jit(solution)/shard_map/all_gather | solution.py:44
  534.3 318.1 %reduce-scatter.15.cloned.1.call-start = ((), (), s32[]{:S(2)}) async-start(), calls=%async_computation.11 | async-start | bytes 19464192
  565.2 419.9 %all-gather.9.cloned.1.call-start = ((), (), s32[]{:S(2)}) async-start(), calls=%async_computation.7 | async-start | bytes 9732096 | tf_op jit(solution)/shard_map/all_gather | solution.py:32
  858.2 163.4 %copy-start.2 = (bf16[1536,512]{1,0:T(8,128)(2,1)S(1)}, bf16[1536,512]{1,0:T(8,128)(2,1)}, u32[]{:S(2)}) copy-start(bf16[1536,512]{1,0:T(8,128)(2,1)} %all-gather.7.cloned.1.call-done) | copy-start | bytes 4718596
  858.2 163.4 %reduce-scatter.11.cloned.1.call-start = ((), (), s32[]{:S(2)}) async-start(), calls=%async_computation.8 | async-start | bytes 1966080 | tf_op jit(solution)/shard_map/reduce_scatter | solution.py:34
  995.2 67.2 %all-gather.11.cloned.1.call-start = ((), (), s32[]{:S(2)}) async-start(), calls=%async_computation.9 | async-start | bytes 1966080 | tf_op jit(solution)/shard_map/all_gather | solution.py:44
Sparse Core Ops, SparseCore 0:
  50.4 289.8 reduce-scatter.12
  346.2 126.7 all-gather.4
  483.2 26.2 reduce-scatter.8
  534.5 15.9 all-gather.6
  565.3 287.1 reduce-scatter.14
  858.3 126.7 all-gather.8
  995.3 26.2 reduce-scatter.10
  1046.4 15.9 all-gather.10
where the time goes:
time: 1070 us
  waiting for transfers between devices  916 us (86%)
  matrix products  49.1 us (5%)
  blocking collectives  42.7 us (4%)
  local copies, waits for them, and re-layouts  41 us (4%)
  between operations  13.6 us (1%)
    unnamed x10, waiting for transfers between devices  577 us
    all_gather x2, waiting for transfers between devices, sublayer(): lax.all_gather(hidden, 'ra', axis=0, tiled=True)  254 us
    reduce_scatter x2, waiting for transfers between devices, sublayer(): lax.psum_scatter(partial_value.astype(jnp.bfloat16), 'cb', scatter_dimens...  52.7 us
    psum x2, blocking collectives, sublayer(): lax.psum((jnp.sum(mixed_rows, axis=1), jnp.sum(mixed_rows * mixed_rows, a...  42.7 us
    all_gather x2, waiting for transfers between devices, sublayer(): return lax.all_gather(normed, 'cb', axis=0, tiled=True)  32 us
    unnamed x14, local copies, waits for them, and re-layouts  30 us
    dot_general x2, matrix products, sublayer(): jnp.dot(stream, paired, preferred_element_type=jnp.float32)  29 us
  transfers between devices with their start and end apart: 8, of which 8 were waited for; matrix products, arithmetic and copies ran while one was open for 0% of the time, Pallas kernels for 0%

commit v1 on v0

v1 whole, which is shorter than its diff:
```python
import jax
import jax.numpy as jnp
from jax import lax
from jax.sharding import PartitionSpec as P

LAYERS = 2
RESIDUAL = 0.5
EPSILON = 1e-05
PAIR = 2
TOKEN_CHUNKS = 2
COLUMN_CHUNKS = 2
BF16 = jnp.bfloat16
F32 = jnp.float32


def dot(a, b):
    return jnp.dot(a, b, preferred_element_type=F32)


def axis_ring(total, stride, size):
    perm = []
    for i in range(total):
        at = (i // stride) % size
        perm.append((i, i + (((at + 1) % size) - at) * stride))
    return perm


def xor_perm(total, bit):
    return [(i, i ^ bit) for i in range(total)]


def swap(x, axis):
    return lax.ppermute(x, axis, xor_perm(lax.axis_size(axis), 1))


def part(x, at, size, dim=0):
    return lax.dynamic_slice_in_dim(x, at * size, size, dim)


def ring_reduce(block, axis, stride, size, me):
    perm = axis_ring(lax.axis_size(axis), stride, size)
    total = block(lax.rem(me + size - 1, size))
    for step in range(1, size):
        arrived = lax.ppermute(total.astype(BF16), axis, perm)
        total = arrived.astype(F32) + block(lax.rem(me + 2 * size - 1 - step, size))
    return total


def ring_gather(x, axis, stride, size, me):
    perm = axis_ring(lax.axis_size(axis), stride, size)
    rows = x.shape[0]
    whole = jnp.zeros((rows * size,) + x.shape[1:], x.dtype)
    whole = lax.dynamic_update_slice_in_dim(whole, x, me * rows, 0)
    for step in range(1, size):
        x = lax.ppermute(x, axis, perm)
        owner = lax.rem(me + size - step, size)
        whole = lax.dynamic_update_slice_in_dim(whole, x, owner * rows, 0)
    return whole


def swap_gather(x, axis, me):
    other = swap(x, axis)
    first = jnp.where(me == 0, x, other)
    second = jnp.where(me == 0, other, x)
    return jnp.concatenate((first, second), axis=0)


def sum_over_ra(stats):
    total = lax.axis_size("ra")
    if total & (total - 1):
        return lax.psum(stats, "ra")
    bit = 1
    while bit < total:
        stats = stats + lax.ppermute(stats, "ra", xor_perm(total, bit))
        bit *= 2
    return stats


def cuts_of(width):
    step = -(-width // COLUMN_CHUNKS)
    step = min(width, -(-step // 128) * 128)
    return [(s, min(step, width - s)) for s in range(0, width, step)]


def per_device(inputs, gate_weight, up_weight, down_weight, norm_gain, norm_shift):
    ra, cb = lax.axis_size("ra"), lax.axis_size("cb")
    r, c = lax.axis_index("ra"), lax.axis_index("cb")
    groups, rows_y = ra // PAIR, cb // 2
    q, g = lax.rem(r, PAIR), r // PAIR
    core, y = lax.rem(c, 2), c // 2
    tokens, width = inputs.shape
    full_width = width * ra
    columns = gate_weight.shape[2]
    half = columns // PAIR
    cuts = cuts_of(half)
    chunk = tokens // TOKEN_CHUNKS

    def weights_of(layer):
        kept, sent = q * half, (1 - q) * half
        pairs, downs = [], []
        for start, size in cuts:
            own = jnp.concatenate(
                [lax.dynamic_slice(w, (layer, 0, kept + start), (1, width, size))[0] for w in (gate_weight, up_weight)], axis=1
            )
            away = jnp.concatenate(
                [lax.dynamic_slice(w, (layer, 0, sent + start), (1, width, size))[0] for w in (gate_weight, up_weight)], axis=1
            )
            pairs.append((own, swap(away, "ra")))
        for start, size in cuts:
            own = lax.dynamic_slice(down_weight, (layer, kept + start, 0), (1, size, width))[0]
            away = lax.dynamic_slice(down_weight, (layer, sent + start, 0), (1, size, width))[0]
            downs.append((own, swap(away, "ra")))
        return pairs, downs

    streams = []
    for k in range(TOKEN_CHUNKS):
        own = inputs[k * chunk:(k + 1) * chunk]
        over = swap(part(own, core, chunk // 2), "ra")
        streams.append((own, swap_gather(over, "cb", core)))

    for layer in range(LAYERS):
        pairs, downs = weights_of(layer)
        last = layer == LAYERS - 1
        after = []
        for own, other in streams:
            block_rows = chunk // groups
            outs_own, outs_other = 0.0, 0.0
            for (w_own, w_other), (d_own, d_other) in zip(pairs, downs):
                size = d_own.shape[0]

                def block(at):
                    return dot(part(own, at, block_rows), w_own) + dot(part(other, at, block_rows), w_other)

                total = ring_reduce(block, "ra", PAIR, groups, g)
                hidden = (jax.nn.silu(total[:, :size]) * total[:, size:]).astype(BF16)
                hidden = ring_gather(hidden, "ra", PAIR, groups, g)
                outs_own = outs_own + dot(hidden, d_own)
                outs_other = outs_other + dot(hidden, d_other)
            out = jnp.concatenate((outs_own, outs_other), axis=1)
            out = part(out, core, chunk // 2) + swap(part(out, 1 - core, chunk // 2).astype(BF16), "cb").astype(F32)
            rows = chunk // cb
            out = ring_reduce(lambda at: part(out, at, rows), "cb", 2, rows_y, y)
            branch = out[:, :width] + swap(out[:, width:].astype(BF16), "ra").astype(F32)
            mine = lax.dynamic_slice_in_dim(own, core * (chunk // 2) + y * rows, rows, 0)
            mixed = RESIDUAL * mine.astype(F32) + branch
            stats = sum_over_ra(jnp.stack((jnp.sum(mixed, axis=1), jnp.sum(mixed * mixed, axis=1))))
            mean = stats[0] / full_width
            var = stats[1] / full_width - mean * mean
            normed = (mixed - mean[:, None]) * lax.rsqrt(var + EPSILON)[:, None]
            normed = (normed * norm_gain[layer] + norm_shift[layer]).astype(BF16)
            if not last:
                normed = jnp.concatenate((normed, swap(normed, "ra")), axis=1)
            whole = swap_gather(ring_gather(normed, "cb", 2, rows_y, y), "cb", core)
            after.append(whole if last else (whole[:, :width], whole[:, width:]))
        streams = after
    return jnp.concatenate(streams, axis=0)


def solution(mesh):
    return jax.shard_map(
        per_device,
        mesh=mesh,
        in_specs=(
            P(None, "ra"),
            P(None, "ra", "cb"),
            P(None, "ra", "cb"),
            P(None, "cb", "ra"),
            P(None, "ra"),
            P(None, "ra"),
        ),
        out_specs=P(None, "ra"),
        check_vma=False,
    )
```

time: 1070 us -> 737 us (0.69); the launches traced: 1070 us -> 727 us
  waiting for transfers between devices: 916 us -> 526 us
  starting transfers between devices: 0.47 us -> 48 us
  blocking collectives: 42.7 us -> 0 us
  matrix products: 49.1 us -> 70.4 us
  local copies, waits for them, and re-layouts: 41 us -> 61.9 us
  between operations: 13.6 us -> 1.92 us
    unnamed x10 -> x0, waiting for transfers between devices: 577 us -> none
    ppermute x0 -> x94, waiting for transfers between devices: none -> 526 us  [the longest x28 263 us: ring_reduce(): arrived = lax.ppermute(total.astype(BF16), axis, perm)]
    all_gather x4 -> x0, waiting for transfers between devices: 286 us -> none  [the longest x2 254 us: sublayer(): lax.all_gather(hidden, 'ra', axis=0, tiled=True)]
    reduce_scatter x2 -> x0, waiting for transfers between devices: 52.7 us -> none  [sublayer(): lax.psum_scatter(partial_value.astype(jnp.bfloat16), 'cb', scatter_dimens...]
    ppermute x0 -> x94, starting transfers between devices: none -> 48 us  [the longest x26 19.4 us: swap(): return lax.ppermute(x, axis, xor_perm(lax.axis_size(axis), 1))]
    psum x2 -> x0, blocking collectives: 42.7 us -> none  [sublayer(): lax.psum((jnp.sum(mixed_rows, axis=1), jnp.sum(mixed_rows * mixed_rows, a...]
    dynamic_update_slice x0 -> x32, local copies, waits for them, and re-layouts: none -> 31.5 us  [the longest x28 16.8 us: ring_gather(): whole = lax.dynamic_update_slice_in_dim(whole, x, owner * rows, 0)]
    dot_general x4 -> x80, matrix products: 49.1 us -> 70.4 us  [dot(): return jnp.dot(a, b, preferred_element_type=F32)]
  transfers between devices with their start and end apart: 8 -> 94, of which waited for: 8 -> 69; matrix products, arithmetic and copies ran while one was open for 0% -> 18% of each run, Pallas kernels for 0% -> 0%
where the time goes in v1:
time: 737 us; the launch traced here: 727 us
  waiting for transfers between devices  526 us (71%)
  matrix products  70.4 us (10%)
  local copies, waits for them, and re-layouts  61.9 us (8%)
  starting transfers between devices  48 us (7%)
  other arithmetic  19 us (3%)
    ppermute x28, waiting for transfers between devices, ring_reduce(): arrived = lax.ppermute(total.astype(BF16), axis, perm)  263 us
    ppermute x28, waiting for transfers between devices, ring_gather(): x = lax.ppermute(x, axis, perm)  154 us
    ppermute x26, waiting for transfers between devices, swap(): return lax.ppermute(x, axis, xor_perm(lax.axis_size(axis), 1))  89.8 us
    dot_general x80, matrix products, dot(): return jnp.dot(a, b, preferred_element_type=F32)  70.4 us
    ppermute x26, starting transfers between devices, swap(): return lax.ppermute(x, axis, xor_perm(lax.axis_size(axis), 1))  19.4 us
    ppermute x12, waiting for transfers between devices, sum_over_ra(): stats = stats + lax.ppermute(stats, 'ra', xor_perm(total, bit))  19.1 us
    dynamic_update_slice x28, local copies, waits for them, and re-layouts, ring_gather(): whole = lax.dynamic_update_slice_in_dim(whole, x, owner * rows, 0)  16.8 us
    dynamic_update_slice x4, local copies, waits for them, and re-layouts, ring_gather(): whole = lax.dynamic_update_slice_in_dim(whole, x, me * rows, 0)  14.7 us
  transfers between devices with their start and end apart: 94, of which 69 were waited for; matrix products, arithmetic and copies ran while one was open for 18% of the time, Pallas kernels for 0%

profile of v1, /device:TPU:0, one launch (start us, length us, event | category | flops | bytes accessed | tf_op | source)
XLA Modules:
  0.0 727.1 jit_solution(12895734027006650525)
XLA Ops:
  2.7 3.0 collective-permute-start
  6.7 5.0 dynamic-slice_bitcast_fusion.1
  15.0 4.6 dynamic-slice_bitcast_fusion.11
  25.2 3.2 fusion.118
  32.7 3.1 fusion.110
  38.1 3.1 fusion.106
  55.1 30.9 %collective-permute-done.9 = bf16[512,1280]{1,0:T(8,128)(2,1)S(1)} collective-permute-done((bf16[512,1280]{1,0:T(8,128)(2,1)}, bf16[512,1280]{1,0:T(8,128)(2,1)S(1)}, u32[]{:S(2)}, u32[]{:S(2)}) %collective-permute-start.9) | collective-permute-done | bytes 1310752 | tf_op jit(solution)/shard_map/ppermute | solution.py:33
  94.0 8.9 %collective-permute-done.59 = bf16[192,1280]{1,0:T(8,128)(2,1)S(1)} collective-permute-done((bf16[192,1280]{1,0:T(8,128)(2,1)S(1)}, bf16[192,1280]{1,0:T(8,128)(2,1)S(1)}, u32[]{:S(2)}, u32[]{:S(2)}) %collective-permute-start.59) | collective-permute-done | bytes 491552 | tf_op jit(solution)/shard_map/ppermute | solution.py:44
  103.6 9.9 %collective-permute-done.10 = bf16[192,1280]{1,0:T(8,128)(2,1)S(1)} collective-permute-done((bf16[192,1280]{1,0:T(8,128)(2,1)S(1)}, bf16[192,1280]{1,0:T(8,128)(2,1)S(1)}, u32[]{:S(2)}, u32[]{:S(2)}) %collective-permute-start.10) | collective-permute-done | bytes 491552 | tf_op jit(solution)/shard_map/ppermute | solution.py:44
  114.5 11.6 %collective-permute-done.53 = bf16[192,1536]{1,0:T(8,128)(2,1)S(1)} collective-permute-done((bf16[192,1536]{1,0:T(8,128)(2,1)S(1)}, bf16[192,1536]{1,0:T(8,128)(2,1)S(1)}, u32[]{:S(2)}, u32[]{:S(2)}) %collective-permute-start.53) | collective-permute-done | bytes 589856 | tf_op jit(solution)/shard_map/ppermute | solution.py:44
  126.8 12.0 %collective-permute-done.3 = bf16[192,1536]{1,0:T(8,128)(2,1)S(1)} collective-permute-done((bf16[192,1536]{1,0:T(8,128)(2,1)S(1)}, bf16[192,1536]{1,0:T(8,128)(2,1)S(1)}, u32[]{:S(2)}, u32[]{:S(2)}) %collective-permute-start.3) | collective-permute-done | bytes 589856 | tf_op jit(solution)/shard_map/ppermute | solution.py:44
  139.4 9.9 %collective-permute-done.60 = bf16[192,1280]{1,0:T(8,128)(2,1)S(1)} collective-permute-done((bf16[192,1280]{1,0:T(8,128)(2,1)S(1)}, bf16[192,1280]{1,0:T(8,128)(2,1)S(1)}, u32[]{:S(2)}, u32[]{:S(2)}) %collective-permute-start.60) | collective-permute-done | bytes 491552 | tf_op jit(solution)/shard_map/ppermute | solution.py:44
  149.9 9.9 %collective-permute-done.11 = bf16[192,1280]{1,0:T(8,128)(2,1)S(1)} collective-permute-done((bf16[192,1280]{1,0:T(8,128)(2,1)S(1)}, bf16[192,1280]{1,0:T(8,128)(2,1)S(1)}, u32[]{:S(2)}, u32[]{:S(2)}) %collective-permute-start.11) | collective-permute-done | bytes 491552 | tf_op jit(solution)/shard_map/ppermute | solution.py:44
  160.4 12.0 %collective-permute-done.54 = bf16[192,1536]{1,0:T(8,128)(2,1)S(1)} collective-permute-done((bf16[192,1536]{1,0:T(8,128)(2,1)S(1)}, bf16[192,1536]{1,0:T(8,128)(2,1)S(1)}, u32[]{:S(2)}, u32[]{:S(2)}) %collective-permute-start.54) | collective-permute-done | bytes 589856 | tf_op jit(solution)/shard_map/ppermute | solution.py:44
  173.1 22.5 %collective-permute-done.61 = bf16[192,1280]{1,0:T(8,128)(2,1)S(1)} collective-permute-done((bf16[192,1280]{1,0:T(8,128)(2,1)S(1)}, bf16[192,1280]{1,0:T(8,128)(2,1)S(1)}, u32[]{:S(2)}, u32[]{:S(2)}) %collective-permute-start.61) | collective-permute-done | bytes 491552 | tf_op jit(solution)/shard_map/ppermute | solution.py:44
  196.5 9.6 %collective-permute-done.12 = bf16[192,1280]{1,0:T(8,128)(2,1)S(1)} collective-permute-done((bf16[192,1280]{1,0:T(8,128)(2,1)S(1)}, bf16[192,1280]{1,0:T(8,128)(2,1)S(1)}, u32[]{:S(2)}, u32[]{:S(2)}) %collective-permute-start.12) | collective-permute-done | bytes 491552 | tf_op jit(solution)/shard_map/ppermute | solution.py:44
  208.7 15.4 %collective-permute-done.62 = bf16[192,640]{1,0:T(8,128)(2,1)S(1)} collective-permute-done((bf16[192,640]{1,0:T(8,128)(2,1)S(1)}, bf16[192,640]{1,0:T(8,128)(2,1)S(1)}, u32[]{:S(2)}, u32[]{:S(2)}) %collective-permute-start.62) | collective-permute-done | bytes 245792 | tf_op jit(solution)/shard_map/ppermute | solution.py:55
  224.7 4.6 collective-permute-done.13
  229.4 5.3 collective-permute-done.63
  234.7 5.2 collective-permute-done.14
  242.5 10.2 %collective-permute-done.5 = bf16[192,1536]{1,0:T(8,128)(2,1)S(1)} collective-permute-done((bf16[192,1536]{1,0:T(8,128)(2,1)S(1)}, bf16[192,1536]{1,0:T(8,128)(2,1)S(1)}, u32[]{:S(2)}, u32[]{:S(2)}) %collective-permute-start.5) | collective-permute-done | bytes 589856 | tf_op jit(solution)/shard_map/ppermute | solution.py:44
  253.6 4.4 collective-permute-done.64
  258.8 4.4 collective-permute-done.15
  265.0 4.6 collective-permute-done.56
  269.5 6.3 collective-permute-done.6
  276.9 5.3 collective-permute-done.57
  282.2 6.3 collective-permute-done.7
  288.6 6.3 collective-permute-done.58
  311.6 11.1 %collective-permute-done.66 = bf16[192,1024]{0,1:T(8,128)(2,1)S(1)} collective-permute-done((bf16[192,1024]{0,1:T(8,128)(2,1)S(1)}, bf16[192,1024]{0,1:T(8,128)(2,1)S(1)}, u32[]{:S(2)}, u32[]{:S(2)}) %collective-permute-start.66) | collective-permute-done | bytes 393248 | tf_op jit(solution)/shard_map/ppermute | solution.py:44
  324.8 8.7 %collective-permute-done.19 = bf16[192,1024]{0,1:T(8,128)(2,1)S(1)} collective-permute-done((bf16[192,1024]{0,1:T(8,128)(2,1)S(1)}, bf16[192,1024]{0,1:T(8,128)(2,1)S(1)}, u32[]{:S(2)}, u32[]{:S(2)}) %collective-permute-start.19) | collective-permute-done | bytes 393248 | tf_op jit(solution)/shard_map/ppermute | solution.py:44
  336.3 5.6 collective-permute-done.20
  355.8 5.0 collective-permute-done.71
  363.3 5.5 dynamic_update_slice.148
  370.2 5.6 dynamic_update_slice.149
  379.1 35.0 %collective-permute-done.24 = bf16[192,512]{0,1:T(8,128)(2,1)S(1)} collective-permute-done((bf16[192,512]{0,1:T(8,128)(2,1)S(1)}, bf16[192,512]{0,1:T(8,128)(2,1)S(1)}, u32[]{:S(2)}, u32[]{:S(2)}) %collective-permute-start.24) | collective-permute-done | bytes 196640 | tf_op jit(solution)/shard_map/ppermute | solution.py:33
  420.4 5.7 dynamic_update_slice.128
  430.0 5.9 dynamic_update_slice.129
  449.6 5.3 collective-permute-done.27
  460.6 6.0 collective-permute-done.35
  467.3 12.0 %collective-permute-done.74 = bf16[192,1536]{1,0:T(8,128)(2,1)S(1)} collective-permute-done((bf16[192,1536]{1,0:T(8,128)(2,1)S(1)}, bf16[192,1536]{1,0:T(8,128)(2,1)S(1)}, u32[]{:S(2)}, u32[]{:S(2)}) %collective-permute-start.74) | collective-permute-done | bytes 589856 | tf_op jit(solution)/shard_map/ppermute | solution.py:44
  479.9 12.0 %collective-permute-done.28 = bf16[192,1536]{1,0:T(8,128)(2,1)S(1)} collective-permute-done((bf16[192,1536]{1,0:T(8,128)(2,1)S(1)}, bf16[192,1536]{1,0:T(8,128)(2,1)S(1)}, u32[]{:S(2)}, u32[]{:S(2)}) %collective-permute-start.28) | collective-permute-done | bytes 589856 | tf_op jit(solution)/shard_map/ppermute | solution.py:44
  492.6 9.9 %collective-permute-done.81 = bf16[192,1280]{1,0:T(8,128)(2,1)S(1)} collective-permute-done((bf16[192,1280]{1,0:T(8,128)(2,1)S(1)}, bf16[192,1280]{1,0:T(8,128)(2,1)S(1)}, u32[]{:S(2)}, u32[]{:S(2)}) %collective-permute-start.81) | collective-permute-done | bytes 491552 | tf_op jit(solution)/shard_map/ppermute | solution.py:44
  503.5 9.5 %collective-permute-done.36 = bf16[192,1280]{1,0:T(8,128)(2,1)S(1)} collective-permute-done((bf16[192,1280]{1,0:T(8,128)(2,1)S(1)}, bf16[192,1280]{1,0:T(8,128)(2,1)S(1)}, u32[]{:S(2)}, u32[]{:S(2)}) %collective-permute-start.36) | collective-permute-done | bytes 491552 | tf_op jit(solution)/shard_map/ppermute | solution.py:44
  513.6 12.0 %collective-permute-done.75 = bf16[192,1536]{1,0:T(8,128)(2,1)S(1)} collective-permute-done((bf16[192,1536]{1,0:T(8,128)(2,1)S(1)}, bf16[192,1536]{1,0:T(8,128)(2,1)S(1)}, u32[]{:S(2)}, u32[]{:S(2)}) %collective-permute-start.75) | collective-permute-done | bytes 589856 | tf_op jit(solution)/shard_map/ppermute | solution.py:44
  526.3 22.5 %collective-permute-done.82 = bf16[192,1280]{1,0:T(8,128)(2,1)S(1)} collective-permute-done((bf16[192,1280]{1,0:T(8,128)(2,1)S(1)}, bf16[192,1280]{1,0:T(8,128)(2,1)S(1)}, u32[]{:S(2)}, u32[]{:S(2)}) %collective-permute-start.82) | collective-permute-done | bytes 491552 | tf_op jit(solution)/shard_map/ppermute | solution.py:44
  549.7 9.6 %collective-permute-done.37 = bf16[192,1280]{1,0:T(8,128)(2,1)S(1)} collective-permute-done((bf16[192,1280]{1,0:T(8,128)(2,1)S(1)}, bf16[192,1280]{1,0:T(8,128)(2,1)S(1)}, u32[]{:S(2)}, u32[]{:S(2)}) %collective-permute-start.37) | collective-permute-done | bytes 491552 | tf_op jit(solution)/shard_map/ppermute | solution.py:44
  561.0 16.3 %collective-permute-done.83 = bf16[192,640]{1,0:T(8,128)(2,1)S(1)} collective-permute-done((bf16[192,640]{1,0:T(8,128)(2,1)S(1)}, bf16[192,640]{1,0:T(8,128)(2,1)S(1)}, u32[]{:S(2)}, u32[]{:S(2)}) %collective-permute-start.83) | collective-permute-done | bytes 245792 | tf_op jit(solution)/shard_map/ppermute | solution.py:55
  577.3 5.2 collective-permute-done.38
  583.6 11.7 %collective-permute-done.30 = bf16[192,1536]{1,0:T(8,128)(2,1)S(1)} collective-permute-done((bf16[192,1536]{1,0:T(8,128)(2,1)S(1)}, bf16[192,1536]{1,0:T(8,128)(2,1)S(1)}, u32[]{:S(2)}, u32[]{:S(2)}) %collective-permute-start.30) | collective-permute-done | bytes 589856 | tf_op jit(solution)/shard_map/ppermute | solution.py:44
  596.2 4.3 collective-permute-done.84
  600.6 5.2 collective-permute-done.39
  605.8 6.3 collective-permute-done.77
  612.1 6.3 collective-permute-done.31
  618.5 5.2 collective-permute-done.85
  624.6 4.4 collective-permute-done.40
  630.7 4.6 collective-permute-done.78
  636.1 5.5 collective-permute-done.32
  641.8 6.1 collective-permute-done.79
  660.6 11.4 %collective-permute-done.87 = bf16[192,1024]{0,1:T(8,128)(2,1)S(1)} collective-permute-done((bf16[192,1024]{0,1:T(8,128)(2,1)S(1)}, bf16[192,1024]{0,1:T(8,128)(2,1)S(1)}, u32[]{:S(2)}, u32[]{:S(2)}) %collective-permute-start.87) | collective-permute-done | bytes 393248 | tf_op jit(solution)/shard_map/ppermute | solution.py:44
  673.1 9.7 %collective-permute-done.44 = bf16[192,1024]{0,1:T(8,128)(2,1)S(1)} collective-permute-done((bf16[192,1024]{0,1:T(8,128)(2,1)S(1)}, bf16[192,1024]{0,1:T(8,128)(2,1)S(1)}, u32[]{:S(2)}, u32[]{:S(2)}) %collective-permute-start.44) | collective-permute-done | bytes 393248 | tf_op jit(solution)/shard_map/ppermute | solution.py:44
  685.6 5.5 collective-permute-done.45
  700.4 2.9 collective-permute-done.48
  706.6 3.4 collective-permute-done.49
  714.8 6.2 collective-permute-done.92
  (435 shorter events, 180.4 us)
Async XLA Ops:
  2.7 48.4 %collective-permute-start = (bf16[384,512]{0,1:T(8,128)(2,1)}, bf16[384,512]{0,1:T(8,128)(2,1)}, u32[]{:S(2)}, u32[]{:S(2)}) collective-permute-start(bf16[384,512]{0,1:T(8,128)(2,1)} %copy.13), channel_id=1, source_target_pairs={{0,4},{4,0},{8,12},{12,8},{16,20},{20,16},{24,28},{28,24},{1,5},{5... | collective-permute-start | bytes 1179656 | tf_op jit(solution)/shard_map/ppermute | solution.py:33
  6.6 44.6 %collective-permute-start.51 = (bf16[384,512]{0,1:T(8,128)(2,1)}, bf16[384,512]{0,1:T(8,128)(2,1)}, u32[]{:S(2)}, u32[]{:S(2)}) collective-permute-start(bf16[384,512]{0,1:T(8,128)(2,1)} %copy.20), channel_id=1, source_target_pairs={{0,4},{4,0},{8,12},{12,8},{16,20},{20,16},{24,28},{28,24},{1,5},{5... | collective-permute-start | bytes 1179656 | tf_op jit(solution)/shard_map/ppermute | solution.py:33
  13.0 78.1 %collective-permute-start.2 = (bf16[512,1536]{1,0:T(8,128)(2,1)}, bf16[512,1536]{1,0:T(8,128)(2,1)S(1)}, u32[]{:S(2)}, u32[]{:S(2)}) collective-permute-start(bf16[512,1536]{1,0:T(8,128)(2,1)} %pad_maximum_fusion.1), channel_id=1, source_target_pairs={{0,4},{4,0},{8,12},{12,8},{16,20},{20,16},{24,28},{28,24},{1,5},{5... | collective-permute-start | bytes 4718600 | tf_op jit(solution)/shard_map/ppermute | solution.py:33
  20.7 65.3 %collective-permute-start.9 = (bf16[512,1280]{1,0:T(8,128)(2,1)}, bf16[512,1280]{1,0:T(8,128)(2,1)S(1)}, u32[]{:S(2)}, u32[]{:S(2)}) collective-permute-start(bf16[512,1280]{1,0:T(8,128)(2,1)} %pad_maximum_fusion.6), channel_id=1, source_target_pairs={{0,4},{4,0},{8,12},{12,8},{16,20},{20,16},{24,28},{28,24},{1,5},{5... | collective-permute-start | bytes 3932168 | tf_op jit(solution)/shard_map/ppermute | solution.py:33
  23.2 234.8 %collective-permute-start.17 = (bf16[640,512]{1,0:T(8,128)(2,1)}, bf16[640,512]{1,0:T(8,128)(2,1)S(1)}, u32[]{:S(2)}, u32[]{:S(2)}) collective-permute-start(bf16[640,512]{1,0:T(8,128)(2,1)} %get-tuple-element.34), channel_id=1, source_target_pairs={{0,4},{4,0},{8,12},{12,8},{16,20},{20,16},{24,28},{28,24},{1,5},{5... | collective-permute-start | bytes 1966088 | tf_op jit(solution)/shard_map/ppermute | solution.py:33
  53.7 241.1 %collective-permute-start.16 = (bf16[768,512]{1,0:T(8,128)(2,1)S(1)}, bf16[768,512]{1,0:T(8,128)(2,1)S(1)}, u32[]{:S(2)}, u32[]{:S(2)}) collective-permute-start(bf16[768,512]{1,0:T(8,128)(2,1)S(1)} %get-tuple-element.32), channel_id=1, source_target_pairs={{0,4},{4,0},{8,12},{12,8},{16,20},{20,16},{24,28},{28,24},{1,5},{5... | collective-permute-start | bytes 2359304 | tf_op jit(solution)/shard_map/ppermute | solution.py:33
  86.7 16.3 %collective-permute-start.59 = (bf16[192,1280]{1,0:T(8,128)(2,1)S(1)}, bf16[192,1280]{1,0:T(8,128)(2,1)S(1)}, u32[]{:S(2)}, u32[]{:S(2)}) collective-permute-start(bf16[192,1280]{1,0:T(8,128)(2,1)S(1)} %fusion.6), channel_id=1, source_target_pairs={{0,8},{4,12},{8,16},{12,20},{16,24},{20,28},{24,0},{28,4},{1,9},{5... | collective-permute-start | bytes 1474568 | tf_op jit(solution)/shard_map/ppermute | solution.py:44
  89.5 24.0 %collective-permute-start.10 = (bf16[192,1280]{1,0:T(8,128)(2,1)S(1)}, bf16[192,1280]{1,0:T(8,128)(2,1)S(1)}, u32[]{:S(2)}, u32[]{:S(2)}) collective-permute-start(bf16[192,1280]{1,0:T(8,128)(2,1)S(1)} %fusion.4), channel_id=1, source_target_pairs={{0,8},{4,12},{8,16},{12,20},{16,24},{20,28},{24,0},{28,4},{1,9},{5... | collective-permute-start | bytes 1474568 | tf_op jit(solution)/shard_map/ppermute | solution.py:44
  91.8 34.4 %collective-permute-start.53 = (bf16[192,1536]{1,0:T(8,128)(2,1)S(1)}, bf16[192,1536]{1,0:T(8,128)(2,1)S(1)}, u32[]{:S(2)}, u32[]{:S(2)}) collective-permute-start(bf16[192,1536]{1,0:T(8,128)(2,1)S(1)} %fusion.2), channel_id=1, source_target_pairs={{0,8},{4,12},{8,16},{12,20},{16,24},{20,28},{24,0},{28,4},{1,9},{5... | collective-permute-start | bytes 1769480 | tf_op jit(solution)/shard_map/ppermute | solution.py:44
  102.9 35.8 %collective-permute-start.3 = (bf16[192,1536]{1,0:T(8,128)(2,1)S(1)}, bf16[192,1536]{1,0:T(8,128)(2,1)S(1)}, u32[]{:S(2)}, u32[]{:S(2)}) collective-permute-start(bf16[192,1536]{1,0:T(8,128)(2,1)S(1)} %fusion), channel_id=1, source_target_pairs={{0,8},{4,12},{8,16},{12,20},{16,24},{20,28},{24,0},{28,4},{1,9},{5... | collective-permute-start | bytes 1769480 | tf_op jit(solution)/shard_map/ppermute | solution.py:44
  113.5 35.8 %collective-permute-start.60 = (bf16[192,1280]{1,0:T(8,128)(2,1)S(1)}, bf16[192,1280]{1,0:T(8,128)(2,1)S(1)}, u32[]{:S(2)}, u32[]{:S(2)}) collective-permute-start(bf16[192,1280]{1,0:T(8,128)(2,1)S(1)} %add_convert_fusion.11), channel_id=1, source_target_pairs={{0,8},{4,12},{8,16},{12,20},{16,24},{20,28},{24,0},{28,4},{1,9},{5... | collective-permute-start | bytes 1474568 | tf_op jit(solution)/shard_map/ppermute | solution.py:44
  126.1 33.7 %collective-permute-start.11 = (bf16[192,1280]{1,0:T(8,128)(2,1)S(1)}, bf16[192,1280]{1,0:T(8,128)(2,1)S(1)}, u32[]{:S(2)}, u32[]{:S(2)}) collective-permute-start(bf16[192,1280]{1,0:T(8,128)(2,1)S(1)} %add_convert_fusion.15), channel_id=1, source_target_pairs={{0,8},{4,12},{8,16},{12,20},{16,24},{20,28},{24,0},{28,4},{1,9},{5... | collective-permute-start | bytes 1474568 | tf_op jit(solution)/shard_map/ppermute | solution.py:44
  138.7 33.7 %collective-permute-start.54 = (bf16[192,1536]{1,0:T(8,128)(2,1)S(1)}, bf16[192,1536]{1,0:T(8,128)(2,1)S(1)}, u32[]{:S(2)}, u32[]{:S(2)}) collective-permute-start(bf16[192,1536]{1,0:T(8,128)(2,1)S(1)} %add_convert_fusion.3), channel_id=1, source_target_pairs={{0,8},{4,12},{8,16},{12,20},{16,24},{20,28},{24,0},{28,4},{1,9},{5... | collective-permute-start | bytes 1769480 | tf_op jit(solution)/shard_map/ppermute | solution.py:44
  149.3 57.8 %collective-permute-start.4 = (bf16[192,1536]{1,0:T(8,128)(2,1)S(1)}, bf16[192,1536]{1,0:T(8,128)(2,1)S(1)}, u32[]{:S(2)}, u32[]{:S(2)}) collective-permute-start(bf16[192,1536]{1,0:T(8,128)(2,1)S(1)} %add_convert_fusion.7), channel_id=1, source_target_pairs={{0,8},{4,12},{8,16},{12,20},{16,24},{20,28},{24,0},{28,4},{1,9},{5... | collective-permute-start | bytes 1769480 | tf_op jit(solution)/shard_map/ppermute | solution.py:44
  159.8 35.8 %collective-permute-start.61 = (bf16[192,1280]{1,0:T(8,128)(2,1)S(1)}, bf16[192,1280]{1,0:T(8,128)(2,1)S(1)}, u32[]{:S(2)}, u32[]{:S(2)}) collective-permute-start(bf16[192,1280]{1,0:T(8,128)(2,1)S(1)} %add_convert_fusion.10), channel_id=1, source_target_pairs={{0,8},{4,12},{8,16},{12,20},{16,24},{20,28},{24,0},{28,4},{1,9},{5... | collective-permute-start | bytes 1474568 | tf_op jit(solution)/shard_map/ppermute | solution.py:44
  172.4 33.7 %collective-permute-start.12 = (bf16[192,1280]{1,0:T(8,128)(2,1)S(1)}, bf16[192,1280]{1,0:T(8,128)(2,1)S(1)}, u32[]{:S(2)}, u32[]{:S(2)}) collective-permute-start(bf16[192,1280]{1,0:T(8,128)(2,1)S(1)} %add_convert_fusion.14), channel_id=1, source_target_pairs={{0,8},{4,12},{8,16},{12,20},{16,24},{20,28},{24,0},{28,4},{1,9},{5... | collective-permute-start | bytes 1474568 | tf_op jit(solution)/shard_map/ppermute | solution.py:44
  195.6 44.4 %collective-permute-start.55 = (bf16[192,1536]{1,0:T(8,128)(2,1)S(1)}, bf16[192,1536]{1,0:T(8,128)(2,1)S(1)}, u32[]{:S(2)}, u32[]{:S(2)}) collective-permute-start(bf16[192,1536]{1,0:T(8,128)(2,1)S(1)} %add_convert_fusion.2), channel_id=1, source_target_pairs={{0,8},{4,12},{8,16},{12,20},{16,24},{20,28},{24,0},{28,4},{1,9},{5... | collective-permute-start | bytes 1769480 | tf_op jit(solution)/shard_map/ppermute | solution.py:44
  206.2 17.9 %collective-permute-start.62 = (bf16[192,640]{1,0:T(8,128)(2,1)S(1)}, bf16[192,640]{1,0:T(8,128)(2,1)S(1)}, u32[]{:S(2)}, u32[]{:S(2)}) collective-permute-start(bf16[192,640]{1,0:T(8,128)(2,1)S(1)} %get-tuple-element.30), channel_id=1, source_target_pairs={{0,8},{4,12},{8,16},{12,20},{16,24},{20,28},{24,0},{28,4},{1,9},{5... | collective-permute-start | bytes 737288 | tf_op jit(solution)/shard_map/ppermute | solution.py:55
  207.1 22.3 %collective-permute-start.13 = (bf16[192,640]{1,0:T(8,128)(2,1)S(1)}, bf16[192,640]{1,0:T(8,128)(2,1)S(1)}, u32[]{:S(2)}, u32[]{:S(2)}) collective-permute-start(bf16[192,640]{1,0:T(8,128)(2,1)S(1)} %get-tuple-element.21), channel_id=1, source_target_pairs={{0,8},{4,12},{8,16},{12,20},{16,24},{20,28},{24,0},{28,4},{1,9},{5... | collective-permute-start | bytes 737288 | tf_op jit(solution)/shard_map/ppermute | solution.py:55
  234.7 18.0 %collective-permute-start.5 = (bf16[192,1536]{1,0:T(8,128)(2,1)S(1)}, bf16[192,1536]{1,0:T(8,128)(2,1)S(1)}, u32[]{:S(2)}, u32[]{:S(2)}) collective-permute-start(bf16[192,1536]{1,0:T(8,128)(2,1)S(1)} %add_convert_fusion.6), channel_id=1, source_target_pairs={{0,8},{4,12},{8,16},{12,20},{16,24},{20,28},{24,0},{28,4},{1,9},{5... | collective-permute-start | bytes 1769480 | tf_op jit(solution)/shard_map/ppermute | solution.py:44
  240.0 18.0 %collective-permute-start.64 = (bf16[192,640]{1,0:T(8,128)(2,1)S(1)}, bf16[192,640]{1,0:T(8,128)(2,1)S(1)}, u32[]{:S(2)}, u32[]{:S(2)}) collective-permute-start(bf16[192,640]{1,0:T(8,128)(2,1)S(1)} %collective-permute-done.63), channel_id=1, source_target_pairs={{0,8},{4,12},{8,16},{12,20},{16,24},{20,28},{24,0},{28,4},{1,9},{5... | collective-permute-start | bytes 737288 | tf_op jit(solution)/shard_map/ppermute | solution.py:55
  240.0 23.2 %collective-permute-start.15 = (bf16[192,640]{1,0:T(8,128)(2,1)S(1)}, bf16[192,640]{1,0:T(8,128)(2,1)S(1)}, u32[]{:S(2)}, u32[]{:S(2)}) collective-permute-start(bf16[192,640]{1,0:T(8,128)(2,1)S(1)} %collective-permute-done.14), channel_id=1, source_target_pairs={{0,8},{4,12},{8,16},{12,20},{16,24},{20,28},{24,0},{28,4},{1,9},{5... | collective-permute-start | bytes 737288 | tf_op jit(solution)/shard_map/ppermute | solution.py:55
  252.7 16.9 %collective-permute-start.56 = (bf16[192,768]{1,0:T(8,128)(2,1)S(1)}, bf16[192,768]{1,0:T(8,128)(2,1)S(1)}, u32[]{:S(2)}, u32[]{:S(2)}) collective-permute-start(bf16[192,768]{1,0:T(8,128)(2,1)S(1)} %get-tuple-element.28), channel_id=1, source_target_pairs={{0,8},{4,12},{8,16},{12,20},{16,24},{20,28},{24,0},{28,4},{1,9},{5... | collective-permute-start | bytes 884744 | tf_op jit(solution)/shard_map/ppermute | solution.py:55
  258.0 17.9 %collective-permute-start.6 = (bf16[192,768]{1,0:T(8,128)(2,1)S(1)}, bf16[192,768]{1,0:T(8,128)(2,1)S(1)}, u32[]{:S(2)}, u32[]{:S(2)}) collective-permute-start(bf16[192,768]{1,0:T(8,128)(2,1)S(1)} %get-tuple-element.19), channel_id=1, source_target_pairs={{0,8},{4,12},{8,16},{12,20},{16,24},{20,28},{24,0},{28,4},{1,9},{5... | collective-permute-start | bytes 884744 | tf_op jit(solution)/shard_map/ppermute | solution.py:55
  269.5 12.6 %collective-permute-start.57 = (bf16[192,768]{1,0:T(8,128)(2,1)S(1)}, bf16[192,768]{1,0:T(8,128)(2,1)S(1)}, u32[]{:S(2)}, u32[]{:S(2)}) collective-permute-start(bf16[192,768]{1,0:T(8,128)(2,1)S(1)} %collective-permute-done.56), channel_id=1, source_target_pairs={{0,8},{4,12},{8,16},{12,20},{16,24},{20,28},{24,0},{28,4},{1,9},{5... | collective-permute-start | bytes 884744 | tf_op jit(solution)/shard_map/ppermute | solution.py:55
  275.9 12.6 %collective-permute-start.7 = (bf16[192,768]{1,0:T(8,128)(2,1)S(1)}, bf16[192,768]{1,0:T(8,128)(2,1)S(1)}, u32[]{:S(2)}, u32[]{:S(2)}) collective-permute-start(bf16[192,768]{1,0:T(8,128)(2,1)S(1)} %collective-permute-done.6), channel_id=1, source_target_pairs={{0,8},{4,12},{8,16},{12,20},{16,24},{20,28},{24,0},{28,4},{1,9},{5... | collective-permute-start | bytes 884744 | tf_op jit(solution)/shard_map/ppermute | solution.py:55
  282.2 12.6 %collective-permute-start.58 = (bf16[192,768]{1,0:T(8,128)(2,1)S(1)}, bf16[192,768]{1,0:T(8,128)(2,1)S(1)}, u32[]{:S(2)}, u32[]{:S(2)}) collective-permute-start(bf16[192,768]{1,0:T(8,128)(2,1)S(1)} %collective-permute-done.57), channel_id=1, source_target_pairs={{0,8},{4,12},{8,16},{12,20},{16,24},{20,28},{24,0},{28,4},{1,9},{5... | collective-permute-start | bytes 884744 | tf_op jit(solution)/shard_map/ppermute | solution.py:55
  307.9 14.9 %collective-permute-start.66 = (bf16[192,1024]{0,1:T(8,128)(2,1)S(1)}, bf16[192,1024]{0,1:T(8,128)(2,1)S(1)}, u32[]{:S(2)}, u32[]{:S(2)}) collective-permute-start(bf16[192,1024]{0,1:T(8,128)(2,1)S(1)} %dynamic-slice_convert_fusion.1), channel_id=1, source_target_pairs={{0,2},{1,3},{2,0},{3,1},{4,6},{5,7},{6,4},{7,5},{8,10},{9,11},{10,... | collective-permute-start | bytes 1179656 | tf_op jit(solution)/shard_map/ppermute | solution.py:44
  311.2 22.4 %collective-permute-start.19 = (bf16[192,1024]{0,1:T(8,128)(2,1)S(1)}, bf16[192,1024]{0,1:T(8,128)(2,1)S(1)}, u32[]{:S(2)}, u32[]{:S(2)}) collective-permute-start(bf16[192,1024]{0,1:T(8,128)(2,1)S(1)} %dynamic-slice_convert_fusion.3), channel_id=1, source_target_pairs={{0,2},{1,3},{2,0},{3,1},{4,6},{5,7},{6,4},{7,5},{8,10},{9,11},{10,... | collective-permute-start | bytes 1179656 | tf_op jit(solution)/shard_map/ppermute | solution.py:44
  323.2 12.3 %collective-permute-start.67 = (bf16[192,512]{0,1:T(8,128)(2,1)S(1)}, bf16[192,512]{0,1:T(8,128)(2,1)S(1)}, u32[]{:S(2)}, u32[]{:S(2)}) collective-permute-start(bf16[192,512]{0,1:T(8,128)(2,1)S(1)} %slice.293), channel_id=1, source_target_pairs={{0,4},{4,0},{8,12},{12,8},{16,20},{20,16},{24,28},{28,24},{1,5},{5... | collective-permute-start | bytes 589832 | tf_op jit(solution)/shard_map/ppermute | solution.py:33
  375.8 60.2 %collective-permute-start.73 = (bf16[384,1024]{0,1:T(8,128)(2,1)}, bf16[384,1024]{0,1:T(8,128)(2,1)}, u32[]{:S(2)}, u32[]{:S(2)}) collective-permute-start(bf16[384,1024]{0,1:T(8,128)(2,1)} %dynamic_update_slice.149), channel_id=1, source_target_pairs={{0,1},{1,0},{2,3},{3,2},{4,5},{5,4},{6,7},{7,6},{8,9},{9,8},{10,11... | collective-permute-start | bytes 2359304 | tf_op jit(solution)/shard_map/ppermute | solution.py:33
  377.0 62.3 %collective-permute-start.34 = (bf16[512,1280]{1,0:T(8,128)(2,1)}, bf16[512,1280]{1,0:T(8,128)(2,1)S(1)}, u32[]{:S(2)}, u32[]{:S(2)}) collective-permute-start(bf16[512,1280]{1,0:T(8,128)(2,1)} %pad_maximum_fusion.8), channel_id=1, source_target_pairs={{0,4},{4,0},{8,12},{12,8},{16,20},{20,16},{24,28},{28,24},{1,5},{5... | collective-permute-start | bytes 3932168 | tf_op jit(solution)/shard_map/ppermute | solution.py:33
  378.4 35.6 %collective-permute-start.24 = (bf16[192,512]{0,1:T(8,128)(2,1)S(1)}, bf16[192,512]{0,1:T(8,128)(2,1)S(1)}, u32[]{:S(2)}, u32[]{:S(2)}) collective-permute-start(bf16[192,512]{0,1:T(8,128)(2,1)S(1)} %get-tuple-element.67), channel_id=1, source_target_pairs={{0,4},{4,0},{8,12},{12,8},{16,20},{20,16},{24,28},{28,24},{1,5},{5... | collective-permute-start | bytes 589832 | tf_op jit(solution)/shard_map/ppermute | solution.py:33
  414.9 13.8 %collective-permute-start.25 = (bf16[192,1024]{0,1:T(8,128)(2,1)}, bf16[192,1024]{0,1:T(8,128)(2,1)}, u32[]{:S(2)}, u32[]{:S(2)}) collective-permute-start(bf16[192,1024]{0,1:T(8,128)(2,1)} %pad_maximum_fusion.9), channel_id=1, source_target_pairs={{0,2},{1,3},{2,0},{3,1},{4,6},{5,7},{6,4},{7,5},{8,10},{9,11},{10,... | collective-permute-start | bytes 1179656 | tf_op jit(solution)/shard_map/ppermute | solution.py:55
  417.4 37.5 %collective-permute-start.27 = (bf16[512,1536]{1,0:T(8,128)(2,1)}, bf16[512,1536]{1,0:T(8,128)(2,1)S(1)}, u32[]{:S(2)}, u32[]{:S(2)}) collective-permute-start(bf16[512,1536]{1,0:T(8,128)(2,1)} %pad_maximum_fusion.3), channel_id=1, source_target_pairs={{0,4},{4,0},{8,12},{12,8},{16,20},{20,16},{24,28},{28,24},{1,5},{5... | collective-permute-start | bytes 4718600 | tf_op jit(solution)/shard_map/ppermute | solution.py:33
  418.9 204.8 %collective-permute-start.42 = (bf16[640,512]{1,0:T(8,128)(2,1)}, bf16[640,512]{1,0:T(8,128)(2,1)S(1)}, u32[]{:S(2)}, u32[]{:S(2)}) collective-permute-start(bf16[640,512]{1,0:T(8,128)(2,1)} %get-tuple-element.33), channel_id=1, source_target_pairs={{0,4},{4,0},{8,12},{12,8},{16,20},{20,16},{24,28},{28,24},{1,5},{5... | collective-permute-start | bytes 1966088 | tf_op jit(solution)/shard_map/ppermute | solution.py:33
  428.7 219.3 %collective-permute-start.41 = (bf16[768,512]{1,0:T(8,128)(2,1)}, bf16[768,512]{1,0:T(8,128)(2,1)}, u32[]{:S(2)}, u32[]{:S(2)}) collective-permute-start(bf16[768,512]{1,0:T(8,128)(2,1)} %get-tuple-element.31), channel_id=1, source_target_pairs={{0,4},{4,0},{8,12},{12,8},{16,20},{20,16},{24,28},{28,24},{1,5},{5... | collective-permute-start | bytes 2359304 | tf_op jit(solution)/shard_map/ppermute | solution.py:33
  440.0 18.8 %collective-permute-start.80 = (bf16[192,1280]{1,0:T(8,128)(2,1)S(1)}, bf16[192,1280]{1,0:T(8,128)(2,1)S(1)}, u32[]{:S(2)}, u32[]{:S(2)}) collective-permute-start(bf16[192,1280]{1,0:T(8,128)(2,1)S(1)} %fusion.7), channel_id=1, source_target_pairs={{0,8},{4,12},{8,16},{12,20},{16,24},{20,28},{24,0},{28,4},{1,9},{5... | collective-permute-start | bytes 1474568 | tf_op jit(solution)/shard_map/ppermute | solution.py:44
  441.8 24.8 %collective-permute-start.35 = (bf16[192,1280]{1,0:T(8,128)(2,1)S(1)}, bf16[192,1280]{1,0:T(8,128)(2,1)S(1)}, u32[]{:S(2)}, u32[]{:S(2)}) collective-permute-start(bf16[192,1280]{1,0:T(8,128)(2,1)S(1)} %fusion.5), channel_id=1, source_target_pairs={{0,8},{4,12},{8,16},{12,20},{16,24},{20,28},{24,0},{28,4},{1,9},{5... | collective-permute-start | bytes 1474568 | tf_op jit(solution)/shard_map/ppermute | solution.py:44
  457.8 21.5 %collective-permute-start.74 = (bf16[192,1536]{1,0:T(8,128)(2,1)S(1)}, bf16[192,1536]{1,0:T(8,128)(2,1)S(1)}, u32[]{:S(2)}, u32[]{:S(2)}) collective-permute-start(bf16[192,1536]{1,0:T(8,128)(2,1)S(1)} %fusion.3), channel_id=1, source_target_pairs={{0,8},{4,12},{8,16},{12,20},{16,24},{20,28},{24,0},{28,4},{1,9},{5... | collective-permute-start | bytes 1769480 | tf_op jit(solution)/shard_map/ppermute | solution.py:44
  458.8 33.1 %collective-permute-start.28 = (bf16[192,1536]{1,0:T(8,128)(2,1)S(1)}, bf16[192,1536]{1,0:T(8,128)(2,1)S(1)}, u32[]{:S(2)}, u32[]{:S(2)}) collective-permute-start(bf16[192,1536]{1,0:T(8,128)(2,1)S(1)} %fusion.1), channel_id=1, source_target_pairs={{0,8},{4,12},{8,16},{12,20},{16,24},{20,28},{24,0},{28,4},{1,9},{5... | collective-permute-start | bytes 1769480 | tf_op jit(solution)/shard_map/ppermute | solution.py:44
  466.7 35.8 %collective-permute-start.81 = (bf16[192,1280]{1,0:T(8,128)(2,1)S(1)}, bf16[192,1280]{1,0:T(8,128)(2,1)S(1)}, u32[]{:S(2)}, u32[]{:S(2)}) collective-permute-start(bf16[192,1280]{1,0:T(8,128)(2,1)S(1)} %add_convert_fusion.9), channel_id=1, source_target_pairs={{0,8},{4,12},{8,16},{12,20},{16,24},{20,28},{24,0},{28,4},{1,9},{5... | collective-permute-start | bytes 1474568 | tf_op jit(solution)/shard_map/ppermute | solution.py:44
  479.3 33.7 %collective-permute-start.36 = (bf16[192,1280]{1,0:T(8,128)(2,1)S(1)}, bf16[192,1280]{1,0:T(8,128)(2,1)S(1)}, u32[]{:S(2)}, u32[]{:S(2)}) collective-permute-start(bf16[192,1280]{1,0:T(8,128)(2,1)S(1)} %add_convert_fusion.13), channel_id=1, source_target_pairs={{0,8},{4,12},{8,16},{12,20},{16,24},{20,28},{24,0},{28,4},{1,9},{5... | collective-permute-start | bytes 1474568 | tf_op jit(solution)/shard_map/ppermute | solution.py:44
  491.9 33.7 %collective-permute-start.75 = (bf16[192,1536]{1,0:T(8,128)(2,1)S(1)}, bf16[192,1536]{1,0:T(8,128)(2,1)S(1)}, u32[]{:S(2)}, u32[]{:S(2)}) collective-permute-start(bf16[192,1536]{1,0:T(8,128)(2,1)S(1)} %add_convert_fusion.1), channel_id=1, source_target_pairs={{0,8},{4,12},{8,16},{12,20},{16,24},{20,28},{24,0},{28,4},{1,9},{5... | collective-permute-start | bytes 1769480 | tf_op jit(solution)/shard_map/ppermute | solution.py:44
  502.5 57.8 %collective-permute-start.29 = (bf16[192,1536]{1,0:T(8,128)(2,1)S(1)}, bf16[192,1536]{1,0:T(8,128)(2,1)S(1)}, u32[]{:S(2)}, u32[]{:S(2)}) collective-permute-start(bf16[192,1536]{1,0:T(8,128)(2,1)S(1)} %add_convert_fusion.5), channel_id=1, source_target_pairs={{0,8},{4,12},{8,16},{12,20},{16,24},{20,28},{24,0},{28,4},{1,9},{5... | collective-permute-start | bytes 1769480 | tf_op jit(solution)/shard_map/ppermute | solution.py:44
  513.0 35.8 %collective-permute-start.82 = (bf16[192,1280]{1,0:T(8,128)(2,1)S(1)}, bf16[192,1280]{1,0:T(8,128)(2,1)S(1)}, u32[]{:S(2)}, u32[]{:S(2)}) collective-permute-start(bf16[192,1280]{1,0:T(8,128)(2,1)S(1)} %add_convert_fusion.8), channel_id=1, source_target_pairs={{0,8},{4,12},{8,16},{12,20},{16,24},{20,28},{24,0},{28,4},{1,9},{5... | collective-permute-start | bytes 1474568 | tf_op jit(solution)/shard_map/ppermute | solution.py:44
  525.6 33.7 %collective-permute-start.37 = (bf16[192,1280]{1,0:T(8,128)(2,1)S(1)}, bf16[192,1280]{1,0:T(8,128)(2,1)S(1)}, u32[]{:S(2)}, u32[]{:S(2)}) collective-permute-start(bf16[192,1280]{1,0:T(8,128)(2,1)S(1)} %add_convert_fusion.12), channel_id=1, source_target_pairs={{0,8},{4,12},{8,16},{12,20},{16,24},{20,28},{24,0},{28,4},{1,9},{5... | collective-permute-start | bytes 1474568 | tf_op jit(solution)/shard_map/ppermute | solution.py:44
  548.8 33.7 %collective-permute-start.76 = (bf16[192,1536]{1,0:T(8,128)(2,1)S(1)}, bf16[192,1536]{1,0:T(8,128)(2,1)S(1)}, u32[]{:S(2)}, u32[]{:S(2)}) collective-permute-start(bf16[192,1536]{1,0:T(8,128)(2,1)S(1)} %add_convert_fusion), channel_id=1, source_target_pairs={{0,8},{4,12},{8,16},{12,20},{16,24},{20,28},{24,0},{28,4},{1,9},{5... | collective-permute-start | bytes 1769480 | tf_op jit(solution)/shard_map/ppermute | solution.py:44
  559.3 17.9 %collective-permute-start.83 = (bf16[192,640]{1,0:T(8,128)(2,1)S(1)}, bf16[192,640]{1,0:T(8,128)(2,1)S(1)}, u32[]{:S(2)}, u32[]{:S(2)}) collective-permute-start(bf16[192,640]{1,0:T(8,128)(2,1)S(1)} %get-tuple-element.26), channel_id=1, source_target_pairs={{0,8},{4,12},{8,16},{12,20},{16,24},{20,28},{24,0},{28,4},{1,9},{5... | collective-permute-start | bytes 737288 | tf_op jit(solution)/shard_map/ppermute | solution.py:55
  560.2 22.3 %collective-permute-start.38 = (bf16[192,640]{1,0:T(8,128)(2,1)S(1)}, bf16[192,640]{1,0:T(8,128)(2,1)S(1)}, u32[]{:S(2)}, u32[]{:S(2)}) collective-permute-start(bf16[192,640]{1,0:T(8,128)(2,1)S(1)} %get-tuple-element.17), channel_id=1, source_target_pairs={{0,8},{4,12},{8,16},{12,20},{16,24},{20,28},{24,0},{28,4},{1,9},{5... | collective-permute-start | bytes 737288 | tf_op jit(solution)/shard_map/ppermute | solution.py:55
  577.3 18.0 %collective-permute-start.30 = (bf16[192,1536]{1,0:T(8,128)(2,1)S(1)}, bf16[192,1536]{1,0:T(8,128)(2,1)S(1)}, u32[]{:S(2)}, u32[]{:S(2)}) collective-permute-start(bf16[192,1536]{1,0:T(8,128)(2,1)S(1)} %add_convert_fusion.4), channel_id=1, source_target_pairs={{0,8},{4,12},{8,16},{12,20},{16,24},{20,28},{24,0},{28,4},{1,9},{5... | collective-permute-start | bytes 1769480 | tf_op jit(solution)/shard_map/ppermute | solution.py:44
  582.5 18.0 %collective-permute-start.84 = (bf16[192,640]{1,0:T(8,128)(2,1)S(1)}, bf16[192,640]{1,0:T(8,128)(2,1)S(1)}, u32[]{:S(2)}, u32[]{:S(2)}) collective-permute-start(bf16[192,640]{1,0:T(8,128)(2,1)S(1)} %collective-permute-done.83), channel_id=1, source_target_pairs={{0,8},{4,12},{8,16},{12,20},{16,24},{20,28},{24,0},{28,4},{1,9},{5... | collective-permute-start | bytes 737288 | tf_op jit(solution)/shard_map/ppermute | solution.py:55
  582.6 23.2 %collective-permute-start.39 = (bf16[192,640]{1,0:T(8,128)(2,1)S(1)}, bf16[192,640]{1,0:T(8,128)(2,1)S(1)}, u32[]{:S(2)}, u32[]{:S(2)}) collective-permute-start(bf16[192,640]{1,0:T(8,128)(2,1)S(1)} %collective-permute-done.38), channel_id=1, source_target_pairs={{0,8},{4,12},{8,16},{12,20},{16,24},{20,28},{24,0},{28,4},{1,9},{5... | collective-permute-start | bytes 737288 | tf_op jit(solution)/shard_map/ppermute | solution.py:55
  595.3 16.9 %collective-permute-start.77 = (bf16[192,768]{1,0:T(8,128)(2,1)S(1)}, bf16[192,768]{1,0:T(8,128)(2,1)S(1)}, u32[]{:S(2)}, u32[]{:S(2)}) collective-permute-start(bf16[192,768]{1,0:T(8,128)(2,1)S(1)} %get-tuple-element.24), channel_id=1, source_target_pairs={{0,8},{4,12},{8,16},{12,20},{16,24},{20,28},{24,0},{28,4},{1,9},{5... | collective-permute-start | bytes 884744 | tf_op jit(solution)/shard_map/ppermute | solution.py:55
  600.5 17.9 %collective-permute-start.31 = (bf16[192,768]{1,0:T(8,128)(2,1)S(1)}, bf16[192,768]{1,0:T(8,128)(2,1)S(1)}, u32[]{:S(2)}, u32[]{:S(2)}) collective-permute-start(bf16[192,768]{1,0:T(8,128)(2,1)S(1)} %get-tuple-element.15), channel_id=1, source_target_pairs={{0,8},{4,12},{8,16},{12,20},{16,24},{20,28},{24,0},{28,4},{1,9},{5... | collective-permute-start | bytes 884744 | tf_op jit(solution)/shard_map/ppermute | solution.py:55
  605.8 17.9 %collective-permute-start.85 = (bf16[192,640]{1,0:T(8,128)(2,1)S(1)}, bf16[192,640]{1,0:T(8,128)(2,1)S(1)}, u32[]{:S(2)}, u32[]{:S(2)}) collective-permute-start(bf16[192,640]{1,0:T(8,128)(2,1)S(1)} %collective-permute-done.84), channel_id=1, source_target_pairs={{0,8},{4,12},{8,16},{12,20},{16,24},{20,28},{24,0},{28,4},{1,9},{5... | collective-permute-start | bytes 737288 | tf_op jit(solution)/shard_map/ppermute | solution.py:55
  612.1 16.9 %collective-permute-start.40 = (bf16[192,640]{1,0:T(8,128)(2,1)S(1)}, bf16[192,640]{1,0:T(8,128)(2,1)S(1)}, u32[]{:S(2)}, u32[]{:S(2)}) collective-permute-start(bf16[192,640]{1,0:T(8,128)(2,1)S(1)} %collective-permute-done.39), channel_id=1, source_target_pairs={{0,8},{4,12},{8,16},{12,20},{16,24},{20,28},{24,0},{28,4},{1,9},{5... | collective-permute-start | bytes 737288 | tf_op jit(solution)/shard_map/ppermute | solution.py:55
  618.4 16.9 %collective-permute-start.78 = (bf16[192,768]{1,0:T(8,128)(2,1)S(1)}, bf16[192,768]{1,0:T(8,128)(2,1)S(1)}, u32[]{:S(2)}, u32[]{:S(2)}) collective-permute-start(bf16[192,768]{1,0:T(8,128)(2,1)S(1)} %collective-permute-done.77), channel_id=1, source_target_pairs={{0,8},{4,12},{8,16},{12,20},{16,24},{20,28},{24,0},{28,4},{1,9},{5... | collective-permute-start | bytes 884744 | tf_op jit(solution)/shard_map/ppermute | solution.py:55
  623.7 17.9 %collective-permute-start.32 = (bf16[192,768]{1,0:T(8,128)(2,1)S(1)}, bf16[192,768]{1,0:T(8,128)(2,1)S(1)}, u32[]{:S(2)}, u32[]{:S(2)}) collective-permute-start(bf16[192,768]{1,0:T(8,128)(2,1)S(1)} %collective-permute-done.31), channel_id=1, source_target_pairs={{0,8},{4,12},{8,16},{12,20},{16,24},{20,28},{24,0},{28,4},{1,9},{5... | collective-permute-start | bytes 884744 | tf_op jit(solution)/shard_map/ppermute | solution.py:55
  635.3 12.6 %collective-permute-start.79 = (bf16[192,768]{1,0:T(8,128)(2,1)S(1)}, bf16[192,768]{1,0:T(8,128)(2,1)S(1)}, u32[]{:S(2)}, u32[]{:S(2)}) collective-permute-start(bf16[192,768]{1,0:T(8,128)(2,1)S(1)} %collective-permute-done.78), channel_id=1, source_target_pairs={{0,8},{4,12},{8,16},{12,20},{16,24},{20,28},{24,0},{28,4},{1,9},{5... | collective-permute-start | bytes 884744 | tf_op jit(solution)/shard_map/ppermute | solution.py:55
  641.6 12.1 %collective-permute-start.33 = (bf16[192,768]{1,0:T(8,128)(2,1)S(1)}, bf16[192,768]{1,0:T(8,128)(2,1)S(1)}, u32[]{:S(2)}, u32[]{:S(2)}) collective-permute-start(bf16[192,768]{1,0:T(8,128)(2,1)S(1)} %collective-permute-done.32), channel_id=1, source_target_pairs={{0,8},{4,12},{8,16},{12,20},{16,24},{20,28},{24,0},{28,4},{1,9},{5... | collective-permute-start | bytes 884744 | tf_op jit(solution)/shard_map/ppermute | solution.py:55
  657.1 14.9 %collective-permute-start.87 = (bf16[192,1024]{0,1:T(8,128)(2,1)S(1)}, bf16[192,1024]{0,1:T(8,128)(2,1)S(1)}, u32[]{:S(2)}, u32[]{:S(2)}) collective-permute-start(bf16[192,1024]{0,1:T(8,128)(2,1)S(1)} %dynamic-slice_convert_fusion), channel_id=1, source_target_pairs={{0,2},{1,3},{2,0},{3,1},{4,6},{5,7},{6,4},{7,5},{8,10},{9,11},{10,... | collective-permute-start | bytes 1179656 | tf_op jit(solution)/shard_map/ppermute | solution.py:44
  659.4 23.4 %collective-permute-start.44 = (bf16[192,1024]{0,1:T(8,128)(2,1)S(1)}, bf16[192,1024]{0,1:T(8,128)(2,1)S(1)}, u32[]{:S(2)}, u32[]{:S(2)}) collective-permute-start(bf16[192,1024]{0,1:T(8,128)(2,1)S(1)} %dynamic-slice_convert_fusion.2), channel_id=1, source_target_pairs={{0,2},{1,3},{2,0},{3,1},{4,6},{5,7},{6,4},{7,5},{8,10},{9,11},{10,... | collective-permute-start | bytes 1179656 | tf_op jit(solution)/shard_map/ppermute | solution.py:44
  672.4 11.5 %collective-permute-start.88 = (bf16[192,512]{0,1:T(8,128)(2,1)S(1)}, bf16[192,512]{0,1:T(8,128)(2,1)S(1)}, u32[]{:S(2)}, u32[]{:S(2)}) collective-permute-start(bf16[192,512]{0,1:T(8,128)(2,1)S(1)} %slice.292), channel_id=1, source_target_pairs={{0,4},{4,0},{8,12},{12,8},{16,20},{20,16},{24,28},{28,24},{1,5},{5... | collective-permute-start | bytes 589832 | tf_op jit(solution)/shard_map/ppermute | solution.py:33
  (79 other events, 629.0 us)

commit v2 on v1

--- a/solution.py
+++ b/solution.py
@@ -7,7 +7,7 @@
 RESIDUAL = 0.5
 EPSILON = 1e-05
 PAIR = 2
-TOKEN_CHUNKS = 2
+TOKEN_CHUNKS = 3
 COLUMN_CHUNKS = 2
 BF16 = jnp.bfloat16
 F32 = jnp.float32
@@ -95,6 +95,14 @@
     cuts = cuts_of(half)
     chunk = tokens // TOKEN_CHUNKS
 
+    queue = [None]
+
+    def queued_swap(away):
+        if queue[0] is not None:
+            away, queue[0] = lax.optimization_barrier((away, queue[0]))
+        queue[0] = swap(away, "ra")
+        return queue[0]
+
     def weights_of(layer):
         kept, sent = q * half, (1 - q) * half
         pairs, downs = [], []
@@ -105,11 +113,11 @@
             away = jnp.concatenate(
                 [lax.dynamic_slice(w, (layer, 0, sent + start), (1, width, size))[0] for w in (gate_weight, up_weight)], axis=1
             )
-            pairs.append((own, swap(away, "ra")))
+            pairs.append((own, queued_swap(away)))
         for start, size in cuts:
             own = lax.dynamic_slice(down_weight, (layer, kept + start, 0), (1, size, width))[0]
             away = lax.dynamic_slice(down_weight, (layer, sent + start, 0), (1, size, width))[0]
-            downs.append((own, swap(away, "ra")))
+            downs.append((own, queued_swap(away)))
         return pairs, downs
 
     streams = []
@@ -118,6 +126,7 @@
         over = swap(part(own, core, chunk // 2), "ra")
         streams.append((own, swap_gather(over, "cb", core)))
 
+    gate_open = None
     for layer in range(LAYERS):
         pairs, downs = weights_of(layer)
         last = layer == LAYERS - 1
@@ -125,6 +134,9 @@
         for own, other in streams:
             block_rows = chunk // groups
             outs_own, outs_other = 0.0, 0.0
+            if gate_open is not None:
+                own, other, _ = lax.optimization_barrier((own, other, gate_open))
+            opened = []
             for (w_own, w_other), (d_own, d_other) in zip(pairs, downs):
                 size = d_own.shape[0]
 
@@ -133,9 +145,11 @@
 
                 total = ring_reduce(block, "ra", PAIR, groups, g)
                 hidden = (jax.nn.silu(total[:, :size]) * total[:, size:]).astype(BF16)
+                opened.append(hidden)
                 hidden = ring_gather(hidden, "ra", PAIR, groups, g)
                 outs_own = outs_own + dot(hidden, d_own)
                 outs_other = outs_other + dot(hidden, d_other)
+            gate_open = tuple(h[:1] for h in opened)
             out = jnp.concatenate((outs_own, outs_other), axis=1)
             out = part(out, core, chunk // 2) + swap(part(out, 1 - core, chunk // 2).astype(BF16), "cb").astype(F32)
             rows = chunk // cb

time: 737 us -> 652 us (0.88)
  waiting for transfers between devices: 526 us -> 450 us
  starting transfers between devices: 48 us -> 75.3 us
  local copies, waits for them, and re-layouts: 61.9 us -> 35.7 us
    ppermute x26 -> x35, waiting for transfers between devices: 89.8 us -> 25.6 us  [swap(): return lax.ppermute(x, axis, xor_perm(lax.axis_size(axis), 1))]
    dynamic_update_slice x28 -> x42, local copies, waits for them, and re-layouts: 16.8 us -> 1.03 us  [ring_gather(): whole = lax.dynamic_update_slice_in_dim(whole, x, owner * rows, 0)]
    dynamic_update_slice x4 -> x0, local copies, waits for them, and re-layouts: 14.7 us -> none  [ring_gather(): whole = lax.dynamic_update_slice_in_dim(whole, x, me * rows, 0)]
    ppermute x12 -> x18, starting transfers between devices: 6.47 us -> 20.8 us  [sum_over_ra(): stats = stats + lax.ppermute(stats, 'ra', xor_perm(total, bit))]
    ppermute x12 -> x18, waiting for transfers between devices: 19.1 us -> 8.13 us  [sum_over_ra(): stats = stats + lax.ppermute(stats, 'ra', xor_perm(total, bit))]
    ppermute x28 -> x42, waiting for transfers between devices: 263 us -> 254 us  [ring_reduce(): arrived = lax.ppermute(total.astype(BF16), axis, perm)]
    ppermute x28 -> x42, waiting for transfers between devices: 154 us -> 163 us  [ring_gather(): x = lax.ppermute(x, axis, perm)]
    ppermute x28 -> x42, starting transfers between devices: 14 us -> 19.8 us  [ring_reduce(): arrived = lax.ppermute(total.astype(BF16), axis, perm)]
  transfers between devices with their start and end apart: 94 -> 137, of which waited for: 69 -> 91; matrix products, arithmetic and copies ran while one was open for 18% -> 16% of each run, Pallas kernels for 0% -> 0%
where the time goes in v2:
time: 652 us; the launch traced here: 643 us
  waiting for transfers between devices  450 us (69%)
  starting transfers between devices  75.3 us (12%)
  matrix products  65.8 us (10%)
  local copies, waits for them, and re-layouts  35.7 us (5%)
  other arithmetic  13.2 us (2%)
    ppermute x42, waiting for transfers between devices, ring_reduce(): arrived = lax.ppermute(total.astype(BF16), axis, perm)  254 us
    ppermute x42, waiting for transfers between devices, ring_gather(): x = lax.ppermute(x, axis, perm)  163 us
    dot_general x120, matrix products, dot(): return jnp.dot(a, b, preferred_element_type=F32)  65.8 us
    ppermute x35, waiting for transfers between devices, swap(): return lax.ppermute(x, axis, xor_perm(lax.axis_size(axis), 1))  25.6 us
    ppermute x35, starting transfers between devices, swap(): return lax.ppermute(x, axis, xor_perm(lax.axis_size(axis), 1))  21.6 us
    ppermute x18, starting transfers between devices, sum_over_ra(): stats = stats + lax.ppermute(stats, 'ra', xor_perm(total, bit))  20.8 us
    ppermute x42, starting transfers between devices, ring_reduce(): arrived = lax.ppermute(total.astype(BF16), axis, perm)  19.8 us
    ppermute x42, starting transfers between devices, ring_gather(): x = lax.ppermute(x, axis, perm)  13.2 us
  transfers between devices with their start and end apart: 137, of which 91 were waited for; matrix products, arithmetic and copies ran while one was open for 16% of the time, Pallas kernels for 0%

profile of v2, /device:TPU:0, one launch (start us, length us, event | category | flops | bytes accessed | tf_op | source)
XLA Modules:
  0.0 642.9 jit_solution(13288860886107505483)
XLA Ops:
  0.0 4.7 dynamic-slice_bitcast_fusion.3
  28.0 4.9 dynamic-slice_bitcast_fusion.11
  51.9 3.9 collective-permute-done.51
  79.1 8.1 %collective-permute-done.3 = bf16[128,1536]{1,0:T(8,128)(2,1)S(1)} collective-permute-done((bf16[128,1536]{1,0:T(8,128)(2,1)S(1)}, bf16[128,1536]{1,0:T(8,128)(2,1)S(1)}, u32[]{:S(2)}, u32[]{:S(2)}) %collective-permute-start.3) | collective-permute-done | bytes 393248 | tf_op jit(solution)/shard_map/ppermute | solution.py:44
  87.7 7.9 %collective-permute-done.53 = bf16[128,1536]{1,0:T(8,128)(2,1)S(1)} collective-permute-done((bf16[128,1536]{1,0:T(8,128)(2,1)S(1)}, bf16[128,1536]{1,0:T(8,128)(2,1)S(1)}, u32[]{:S(2)}, u32[]{:S(2)}) %collective-permute-start.53) | collective-permute-done | bytes 393248 | tf_op jit(solution)/shard_map/ppermute | solution.py:44
  96.4 7.7 %collective-permute-done.96 = bf16[128,1536]{1,0:T(8,128)(2,1)S(1)} collective-permute-done((bf16[128,1536]{1,0:T(8,128)(2,1)S(1)}, bf16[128,1536]{1,0:T(8,128)(2,1)S(1)}, u32[]{:S(2)}, u32[]{:S(2)}) %collective-permute-start.96) | collective-permute-done | bytes 393248 | tf_op jit(solution)/shard_map/ppermute | solution.py:44
  104.6 7.9 %collective-permute-done.4 = bf16[128,1536]{1,0:T(8,128)(2,1)S(1)} collective-permute-done((bf16[128,1536]{1,0:T(8,128)(2,1)S(1)}, bf16[128,1536]{1,0:T(8,128)(2,1)S(1)}, u32[]{:S(2)}, u32[]{:S(2)}) %collective-permute-start.4) | collective-permute-done | bytes 393248 | tf_op jit(solution)/shard_map/ppermute | solution.py:44
  113.0 7.9 %collective-permute-done.54 = bf16[128,1536]{1,0:T(8,128)(2,1)S(1)} collective-permute-done((bf16[128,1536]{1,0:T(8,128)(2,1)S(1)}, bf16[128,1536]{1,0:T(8,128)(2,1)S(1)}, u32[]{:S(2)}, u32[]{:S(2)}) %collective-permute-start.54) | collective-permute-done | bytes 393248 | tf_op jit(solution)/shard_map/ppermute | solution.py:44
  121.4 7.9 %collective-permute-done.97 = bf16[128,1536]{1,0:T(8,128)(2,1)S(1)} collective-permute-done((bf16[128,1536]{1,0:T(8,128)(2,1)S(1)}, bf16[128,1536]{1,0:T(8,128)(2,1)S(1)}, u32[]{:S(2)}, u32[]{:S(2)}) %collective-permute-start.97) | collective-permute-done | bytes 393248 | tf_op jit(solution)/shard_map/ppermute | solution.py:44
  129.8 7.9 %collective-permute-done.5 = bf16[128,1536]{1,0:T(8,128)(2,1)S(1)} collective-permute-done((bf16[128,1536]{1,0:T(8,128)(2,1)S(1)}, bf16[128,1536]{1,0:T(8,128)(2,1)S(1)}, u32[]{:S(2)}, u32[]{:S(2)}) %collective-permute-start.5) | collective-permute-done | bytes 393248 | tf_op jit(solution)/shard_map/ppermute | solution.py:44
  138.5 7.7 %collective-permute-done.55 = bf16[128,1536]{1,0:T(8,128)(2,1)S(1)} collective-permute-done((bf16[128,1536]{1,0:T(8,128)(2,1)S(1)}, bf16[128,1536]{1,0:T(8,128)(2,1)S(1)}, u32[]{:S(2)}, u32[]{:S(2)}) %collective-permute-start.55) | collective-permute-done | bytes 393248 | tf_op jit(solution)/shard_map/ppermute | solution.py:44
  146.9 7.8 %collective-permute-done.98 = bf16[128,1536]{1,0:T(8,128)(2,1)S(1)} collective-permute-done((bf16[128,1536]{1,0:T(8,128)(2,1)S(1)}, bf16[128,1536]{1,0:T(8,128)(2,1)S(1)}, u32[]{:S(2)}, u32[]{:S(2)}) %collective-permute-start.98) | collective-permute-done | bytes 393248 | tf_op jit(solution)/shard_map/ppermute | solution.py:44
  163.1 4.2 collective-permute-done.99
  167.3 18.2 %collective-permute-done.7 = bf16[128,768]{1,0:T(8,128)(2,1)S(1)} collective-permute-done((bf16[128,768]{1,0:T(8,128)(2,1)S(1)}, bf16[128,768]{1,0:T(8,128)(2,1)S(1)}, u32[]{:S(2)}, u32[]{:S(2)}) %collective-permute-start.7) | collective-permute-done | bytes 196640 | tf_op jit(solution)/shard_map/ppermute | solution.py:55
  185.6 3.9 collective-permute-done.57
  189.5 4.1 collective-permute-done.100
  197.8 4.0 collective-permute-done.102
  202.2 3.8 collective-permute-done.8
  206.1 4.2 collective-permute-done.58
  210.3 4.2 collective-permute-done.101
  214.5 7.0 %collective-permute-done.11 = bf16[128,1280]{1,0:T(8,128)(2,1)S(1)} collective-permute-done((bf16[128,1280]{1,0:T(8,128)(2,1)S(1)}, bf16[128,1280]{1,0:T(8,128)(2,1)S(1)}, u32[]{:S(2)}, u32[]{:S(2)}) %collective-permute-start.11) | collective-permute-done | bytes 327712 | tf_op jit(solution)/shard_map/ppermute | solution.py:44
  222.0 6.6 %collective-permute-done.60 = bf16[128,1280]{1,0:T(8,128)(2,1)S(1)} collective-permute-done((bf16[128,1280]{1,0:T(8,128)(2,1)S(1)}, bf16[128,1280]{1,0:T(8,128)(2,1)S(1)}, u32[]{:S(2)}, u32[]{:S(2)}) %collective-permute-start.60) | collective-permute-done | bytes 327712 | tf_op jit(solution)/shard_map/ppermute | solution.py:44
  229.0 6.5 %collective-permute-done.103 = bf16[128,1280]{1,0:T(8,128)(2,1)S(1)} collective-permute-done((bf16[128,1280]{1,0:T(8,128)(2,1)S(1)}, bf16[128,1280]{1,0:T(8,128)(2,1)S(1)}, u32[]{:S(2)}, u32[]{:S(2)}) %collective-permute-start.103) | collective-permute-done | bytes 327712 | tf_op jit(solution)/shard_map/ppermute | solution.py:44
  236.4 6.2 collective-permute-done.12
  243.2 6.4 collective-permute-done.61
  250.2 6.4 collective-permute-done.104
  263.7 3.5 collective-permute-done.105
  295.0 5.1 collective-permute-done.19
  300.5 5.2 collective-permute-done.66
  306.2 4.2 collective-permute-done.109
  310.9 6.8 %collective-permute-done.20 = bf16[128,512]{0,1:T(8,128)(2,1)S(1)} collective-permute-done((bf16[128,512]{0,1:T(8,128)(2,1)S(1)}, bf16[128,512]{0,1:T(8,128)(2,1)S(1)}, u32[]{:S(2)}, u32[]{:S(2)}) %collective-permute-start.20) | collective-permute-done | bytes 131104 | tf_op jit(solution)/shard_map/ppermute | solution.py:33
  335.2 5.0 collective-permute-done.114
  349.1 4.8 collective-permute-done.72
  354.1 4.0 collective-permute-done.25
  376.4 8.1 %collective-permute-done.117 = bf16[128,1536]{1,0:T(8,128)(2,1)S(1)} collective-permute-done((bf16[128,1536]{1,0:T(8,128)(2,1)S(1)}, bf16[128,1536]{1,0:T(8,128)(2,1)S(1)}, u32[]{:S(2)}, u32[]{:S(2)}) %collective-permute-start.117) | collective-permute-done | bytes 393248 | tf_op jit(solution)/shard_map/ppermute | solution.py:44
  385.0 7.9 %collective-permute-done.74 = bf16[128,1536]{1,0:T(8,128)(2,1)S(1)} collective-permute-done((bf16[128,1536]{1,0:T(8,128)(2,1)S(1)}, bf16[128,1536]{1,0:T(8,128)(2,1)S(1)}, u32[]{:S(2)}, u32[]{:S(2)}) %collective-permute-start.74) | collective-permute-done | bytes 393248 | tf_op jit(solution)/shard_map/ppermute | solution.py:44
  393.4 7.9 %collective-permute-done.28 = bf16[128,1536]{1,0:T(8,128)(2,1)S(1)} collective-permute-done((bf16[128,1536]{1,0:T(8,128)(2,1)S(1)}, bf16[128,1536]{1,0:T(8,128)(2,1)S(1)}, u32[]{:S(2)}, u32[]{:S(2)}) %collective-permute-start.28) | collective-permute-done | bytes 393248 | tf_op jit(solution)/shard_map/ppermute | solution.py:44
  401.9 7.9 %collective-permute-done.118 = bf16[128,1536]{1,0:T(8,128)(2,1)S(1)} collective-permute-done((bf16[128,1536]{1,0:T(8,128)(2,1)S(1)}, bf16[128,1536]{1,0:T(8,128)(2,1)S(1)}, u32[]{:S(2)}, u32[]{:S(2)}) %collective-permute-start.118) | collective-permute-done | bytes 393248 | tf_op jit(solution)/shard_map/ppermute | solution.py:44
  410.3 7.9 %collective-permute-done.75 = bf16[128,1536]{1,0:T(8,128)(2,1)S(1)} collective-permute-done((bf16[128,1536]{1,0:T(8,128)(2,1)S(1)}, bf16[128,1536]{1,0:T(8,128)(2,1)S(1)}, u32[]{:S(2)}, u32[]{:S(2)}) %collective-permute-start.75) | collective-permute-done | bytes 393248 | tf_op jit(solution)/shard_map/ppermute | solution.py:44
  418.7 7.9 %collective-permute-done.29 = bf16[128,1536]{1,0:T(8,128)(2,1)S(1)} collective-permute-done((bf16[128,1536]{1,0:T(8,128)(2,1)S(1)}, bf16[128,1536]{1,0:T(8,128)(2,1)S(1)}, u32[]{:S(2)}, u32[]{:S(2)}) %collective-permute-start.29) | collective-permute-done | bytes 393248 | tf_op jit(solution)/shard_map/ppermute | solution.py:44
  430.0 5.1 collective-permute-done.119
  435.7 7.8 %collective-permute-done.76 = bf16[128,1536]{1,0:T(8,128)(2,1)S(1)} collective-permute-done((bf16[128,1536]{1,0:T(8,128)(2,1)S(1)}, bf16[128,1536]{1,0:T(8,128)(2,1)S(1)}, u32[]{:S(2)}, u32[]{:S(2)}) %collective-permute-start.76) | collective-permute-done | bytes 393248 | tf_op jit(solution)/shard_map/ppermute | solution.py:44
  443.9 8.0 %collective-permute-done.30 = bf16[128,1536]{1,0:T(8,128)(2,1)S(1)} collective-permute-done((bf16[128,1536]{1,0:T(8,128)(2,1)S(1)}, bf16[128,1536]{1,0:T(8,128)(2,1)S(1)}, u32[]{:S(2)}, u32[]{:S(2)}) %collective-permute-start.30) | collective-permute-done | bytes 393248 | tf_op jit(solution)/shard_map/ppermute | solution.py:44
  452.7 6.2 collective-permute-done.123
  459.3 6.6 %collective-permute-done.80 = bf16[128,1280]{1,0:T(8,128)(2,1)S(1)} collective-permute-done((bf16[128,1280]{1,0:T(8,128)(2,1)S(1)}, bf16[128,1280]{1,0:T(8,128)(2,1)S(1)}, u32[]{:S(2)}, u32[]{:S(2)}) %collective-permute-start.80) | collective-permute-done | bytes 327712 | tf_op jit(solution)/shard_map/ppermute | solution.py:44
  466.4 6.6 %collective-permute-done.35 = bf16[128,1280]{1,0:T(8,128)(2,1)S(1)} collective-permute-done((bf16[128,1280]{1,0:T(8,128)(2,1)S(1)}, bf16[128,1280]{1,0:T(8,128)(2,1)S(1)}, u32[]{:S(2)}, u32[]{:S(2)}) %collective-permute-start.35) | collective-permute-done | bytes 327712 | tf_op jit(solution)/shard_map/ppermute | solution.py:44
  473.4 3.8 collective-permute-done.120
  477.3 4.2 collective-permute-done.77
  481.5 4.2 collective-permute-done.31
  485.7 18.2 %collective-permute-done.121 = bf16[128,768]{1,0:T(8,128)(2,1)S(1)} collective-permute-done((bf16[128,768]{1,0:T(8,128)(2,1)S(1)}, bf16[128,768]{1,0:T(8,128)(2,1)S(1)}, u32[]{:S(2)}, u32[]{:S(2)}) %collective-permute-start.121) | collective-permute-done | bytes 196640 | tf_op jit(solution)/shard_map/ppermute | solution.py:55
  503.9 3.9 collective-permute-done.78
  507.9 4.2 collective-permute-done.32
  515.0 5.2 collective-permute-done.36
  520.6 3.8 collective-permute-done.122
  524.5 4.2 collective-permute-done.79
  528.7 4.2 collective-permute-done.33
  534.0 5.9 collective-permute-done.125
  540.5 6.4 collective-permute-done.82
  547.5 6.4 collective-permute-done.37
  592.3 5.1 collective-permute-done.130
  598.6 4.4 collective-permute-done.87
  604.2 3.5 collective-permute-done.44
  628.1 4.5 collective-permute-done.49
  634.4 4.5 collective-permute-done.92
  (598 shorter events, 246.5 us)
Async XLA Ops:
  6.0 65.1 %collective-permute-start.2 = (bf16[512,1536]{1,0:T(8,128)(2,1)}, bf16[512,1536]{1,0:T(8,128)(2,1)S(1)}, u32[]{:S(2)}, u32[]{:S(2)}) collective-permute-start(bf16[512,1536]{1,0:T(8,128)(2,1)} %pad_maximum_fusion.1), channel_id=1, source_target_pairs={{0,4},{4,0},{8,12},{12,8},{16,20},{20,16},{24,28},{28,24},{1,5},{5... | collective-permute-start | bytes 4718600 | tf_op jit(solution)/shard_map/ppermute | solution.py:33
  13.4 43.7 %collective-permute-start = (bf16[256,512]{0,1:T(8,128)(2,1)}, bf16[256,512]{0,1:T(8,128)(2,1)}, u32[]{:S(2)}, u32[]{:S(2)}) collective-permute-start(bf16[256,512]{0,1:T(8,128)(2,1)} %copy.14), channel_id=1, source_target_pairs={{0,4},{4,0},{8,12},{12,8},{16,20},{20,16},{24,28},{28,24},{1,5},{5... | collective-permute-start | bytes 786440 | tf_op jit(solution)/shard_map/ppermute | solution.py:33
  17.1 38.7 %collective-permute-start.51 = (bf16[256,512]{0,1:T(8,128)(2,1)}, bf16[256,512]{0,1:T(8,128)(2,1)}, u32[]{:S(2)}, u32[]{:S(2)}) collective-permute-start(bf16[256,512]{0,1:T(8,128)(2,1)} %constant_dynamic-slice_fusion.1), channel_id=1, source_target_pairs={{0,4},{4,0},{8,12},{12,8},{16,20},{20,16},{24,28},{28,24},{1,5},{5... | collective-permute-start | bytes 786440 | tf_op jit(solution)/shard_map/ppermute | solution.py:33
  22.8 37.7 %collective-permute-start.94 = (bf16[256,512]{0,1:T(8,128)(2,1)}, bf16[256,512]{0,1:T(8,128)(2,1)}, u32[]{:S(2)}, u32[]{:S(2)}) collective-permute-start(bf16[256,512]{0,1:T(8,128)(2,1)} %constant_dynamic-slice_fusion), channel_id=1, source_target_pairs={{0,4},{4,0},{8,12},{12,8},{16,20},{20,16},{24,28},{28,24},{1,5},{5... | collective-permute-start | bytes 786440 | tf_op jit(solution)/shard_map/ppermute | solution.py:33
  71.1 84.2 %collective-permute-start.9 = (bf16[512,1280]{1,0:T(8,128)(2,1)S(1)}, bf16[512,1280]{1,0:T(8,128)(2,1)S(1)}, u32[]{:S(2)}, u32[]{:S(2)}) collective-permute-start(bf16[512,1280]{1,0:T(8,128)(2,1)S(1)} %pad_maximum_fusion.5), channel_id=1, source_target_pairs={{0,4},{4,0},{8,12},{12,8},{16,20},{20,16},{24,28},{28,24},{1,5},{5... | collective-permute-start | bytes 3932168 | tf_op jit(solution)/shard_map/ppermute | solution.py:33
  73.4 13.8 %collective-permute-start.3 = (bf16[128,1536]{1,0:T(8,128)(2,1)S(1)}, bf16[128,1536]{1,0:T(8,128)(2,1)S(1)}, u32[]{:S(2)}, u32[]{:S(2)}) collective-permute-start(bf16[128,1536]{1,0:T(8,128)(2,1)S(1)} %fusion), channel_id=1, source_target_pairs={{0,8},{4,12},{8,16},{12,20},{16,24},{20,28},{24,0},{28,4},{1,9},{5... | collective-permute-start | bytes 1179656 | tf_op jit(solution)/shard_map/ppermute | solution.py:44
  75.4 20.2 %collective-permute-start.53 = (bf16[128,1536]{1,0:T(8,128)(2,1)S(1)}, bf16[128,1536]{1,0:T(8,128)(2,1)S(1)}, u32[]{:S(2)}, u32[]{:S(2)}) collective-permute-start(bf16[128,1536]{1,0:T(8,128)(2,1)S(1)} %fusion.2), channel_id=1, source_target_pairs={{0,8},{4,12},{8,16},{12,20},{16,24},{20,28},{24,0},{28,4},{1,9},{5... | collective-permute-start | bytes 1179656 | tf_op jit(solution)/shard_map/ppermute | solution.py:44
  77.5 26.6 %collective-permute-start.96 = (bf16[128,1536]{1,0:T(8,128)(2,1)S(1)}, bf16[128,1536]{1,0:T(8,128)(2,1)S(1)}, u32[]{:S(2)}, u32[]{:S(2)}) collective-permute-start(bf16[128,1536]{1,0:T(8,128)(2,1)S(1)} %fusion.4), channel_id=1, source_target_pairs={{0,8},{4,12},{8,16},{12,20},{16,24},{20,28},{24,0},{28,4},{1,9},{5... | collective-permute-start | bytes 1179656 | tf_op jit(solution)/shard_map/ppermute | solution.py:44
  87.7 24.8 %collective-permute-start.4 = (bf16[128,1536]{1,0:T(8,128)(2,1)S(1)}, bf16[128,1536]{1,0:T(8,128)(2,1)S(1)}, u32[]{:S(2)}, u32[]{:S(2)}) collective-permute-start(bf16[128,1536]{1,0:T(8,128)(2,1)S(1)} %add_convert_fusion.11), channel_id=1, source_target_pairs={{0,8},{4,12},{8,16},{12,20},{16,24},{20,28},{24,0},{28,4},{1,9},{5... | collective-permute-start | bytes 1179656 | tf_op jit(solution)/shard_map/ppermute | solution.py:44
  96.1 24.9 %collective-permute-start.54 = (bf16[128,1536]{1,0:T(8,128)(2,1)S(1)}, bf16[128,1536]{1,0:T(8,128)(2,1)S(1)}, u32[]{:S(2)}, u32[]{:S(2)}) collective-permute-start(bf16[128,1536]{1,0:T(8,128)(2,1)S(1)} %add_convert_fusion.7), channel_id=1, source_target_pairs={{0,8},{4,12},{8,16},{12,20},{16,24},{20,28},{24,0},{28,4},{1,9},{5... | collective-permute-start | bytes 1179656 | tf_op jit(solution)/shard_map/ppermute | solution.py:44
  104.5 24.9 %collective-permute-start.97 = (bf16[128,1536]{1,0:T(8,128)(2,1)S(1)}, bf16[128,1536]{1,0:T(8,128)(2,1)S(1)}, u32[]{:S(2)}, u32[]{:S(2)}) collective-permute-start(bf16[128,1536]{1,0:T(8,128)(2,1)S(1)} %add_convert_fusion.3), channel_id=1, source_target_pairs={{0,8},{4,12},{8,16},{12,20},{16,24},{20,28},{24,0},{28,4},{1,9},{5... | collective-permute-start | bytes 1179656 | tf_op jit(solution)/shard_map/ppermute | solution.py:44
  112.9 24.8 %collective-permute-start.5 = (bf16[128,1536]{1,0:T(8,128)(2,1)S(1)}, bf16[128,1536]{1,0:T(8,128)(2,1)S(1)}, u32[]{:S(2)}, u32[]{:S(2)}) collective-permute-start(bf16[128,1536]{1,0:T(8,128)(2,1)S(1)} %add_convert_fusion.10), channel_id=1, source_target_pairs={{0,8},{4,12},{8,16},{12,20},{16,24},{20,28},{24,0},{28,4},{1,9},{5... | collective-permute-start | bytes 1179656 | tf_op jit(solution)/shard_map/ppermute | solution.py:44
  121.3 24.9 %collective-permute-start.55 = (bf16[128,1536]{1,0:T(8,128)(2,1)S(1)}, bf16[128,1536]{1,0:T(8,128)(2,1)S(1)}, u32[]{:S(2)}, u32[]{:S(2)}) collective-permute-start(bf16[128,1536]{1,0:T(8,128)(2,1)S(1)} %add_convert_fusion.6), channel_id=1, source_target_pairs={{0,8},{4,12},{8,16},{12,20},{16,24},{20,28},{24,0},{28,4},{1,9},{5... | collective-permute-start | bytes 1179656 | tf_op jit(solution)/shard_map/ppermute | solution.py:44
  129.8 24.9 %collective-permute-start.98 = (bf16[128,1536]{1,0:T(8,128)(2,1)S(1)}, bf16[128,1536]{1,0:T(8,128)(2,1)S(1)}, u32[]{:S(2)}, u32[]{:S(2)}) collective-permute-start(bf16[128,1536]{1,0:T(8,128)(2,1)S(1)} %add_convert_fusion.2), channel_id=1, source_target_pairs={{0,8},{4,12},{8,16},{12,20},{16,24},{20,28},{24,0},{28,4},{1,9},{5... | collective-permute-start | bytes 1179656 | tf_op jit(solution)/shard_map/ppermute | solution.py:44
  138.4 20.4 %collective-permute-start.6 = (bf16[128,768]{1,0:T(8,128)(2,1)S(1)}, bf16[128,768]{1,0:T(8,128)(2,1)S(1)}, u32[]{:S(2)}, u32[]{:S(2)}) collective-permute-start(bf16[128,768]{1,0:T(8,128)(2,1)S(1)} %get-tuple-element.83), channel_id=1, source_target_pairs={{0,8},{4,12},{8,16},{12,20},{16,24},{20,28},{24,0},{28,4},{1,9},{5... | collective-permute-start | bytes 589832 | tf_op jit(solution)/shard_map/ppermute | solution.py:55
  146.8 16.2 %collective-permute-start.56 = (bf16[128,768]{1,0:T(8,128)(2,1)S(1)}, bf16[128,768]{1,0:T(8,128)(2,1)S(1)}, u32[]{:S(2)}, u32[]{:S(2)}) collective-permute-start(bf16[128,768]{1,0:T(8,128)(2,1)S(1)} %get-tuple-element.72), channel_id=1, source_target_pairs={{0,8},{4,12},{8,16},{12,20},{16,24},{20,28},{24,0},{28,4},{1,9},{5... | collective-permute-start | bytes 589832 | tf_op jit(solution)/shard_map/ppermute | solution.py:55
  156.5 37.2 %collective-permute-start.10 = (bf16[128,1280]{1,0:T(8,128)(2,1)S(1)}, bf16[128,1280]{1,0:T(8,128)(2,1)S(1)}, u32[]{:S(2)}, u32[]{:S(2)}) collective-permute-start(bf16[128,1280]{1,0:T(8,128)(2,1)S(1)} %fusion.6), channel_id=1, source_target_pairs={{0,8},{4,12},{8,16},{12,20},{16,24},{20,28},{24,0},{28,4},{1,9},{5... | collective-permute-start | bytes 983048 | tf_op jit(solution)/shard_map/ppermute | solution.py:44
  157.1 78.9 %collective-permute-start.16 = (bf16[768,512]{1,0:T(8,128)(2,1)S(1)}, bf16[768,512]{1,0:T(8,128)(2,1)S(1)}, u32[]{:S(2)}, u32[]{:S(2)}) collective-permute-start(bf16[768,512]{1,0:T(8,128)(2,1)S(1)} %copy-done.18), channel_id=1, source_target_pairs={{0,4},{4,0},{8,12},{12,8},{16,20},{20,16},{24,28},{28,24},{1,5},{5... | collective-permute-start | bytes 2359304 | tf_op jit(solution)/shard_map/ppermute | solution.py:33
  158.8 36.9 %collective-permute-start.59 = (bf16[128,1280]{1,0:T(8,128)(2,1)S(1)}, bf16[128,1280]{1,0:T(8,128)(2,1)S(1)}, u32[]{:S(2)}, u32[]{:S(2)}) collective-permute-start(bf16[128,1280]{1,0:T(8,128)(2,1)S(1)} %fusion.8), channel_id=1, source_target_pairs={{0,8},{4,12},{8,16},{12,20},{16,24},{20,28},{24,0},{28,4},{1,9},{5... | collective-permute-start | bytes 983048 | tf_op jit(solution)/shard_map/ppermute | solution.py:44
  163.1 22.5 %collective-permute-start.7 = (bf16[128,768]{1,0:T(8,128)(2,1)S(1)}, bf16[128,768]{1,0:T(8,128)(2,1)S(1)}, u32[]{:S(2)}, u32[]{:S(2)}) collective-permute-start(bf16[128,768]{1,0:T(8,128)(2,1)S(1)} %collective-permute-done.6), channel_id=1, source_target_pairs={{0,8},{4,12},{8,16},{12,20},{16,24},{20,28},{24,0},{28,4},{1,9},{5... | collective-permute-start | bytes 589832 | tf_op jit(solution)/shard_map/ppermute | solution.py:55
  167.3 22.2 %collective-permute-start.57 = (bf16[128,768]{1,0:T(8,128)(2,1)S(1)}, bf16[128,768]{1,0:T(8,128)(2,1)S(1)}, u32[]{:S(2)}, u32[]{:S(2)}) collective-permute-start(bf16[128,768]{1,0:T(8,128)(2,1)S(1)} %collective-permute-done.56), channel_id=1, source_target_pairs={{0,8},{4,12},{8,16},{12,20},{16,24},{20,28},{24,0},{28,4},{1,9},{5... | collective-permute-start | bytes 589832 | tf_op jit(solution)/shard_map/ppermute | solution.py:55
  193.7 16.5 %collective-permute-start.58 = (bf16[128,768]{1,0:T(8,128)(2,1)S(1)}, bf16[128,768]{1,0:T(8,128)(2,1)S(1)}, u32[]{:S(2)}, u32[]{:S(2)}) collective-permute-start(bf16[128,768]{1,0:T(8,128)(2,1)S(1)} %collective-permute-done.57), channel_id=1, source_target_pairs={{0,8},{4,12},{8,16},{12,20},{16,24},{20,28},{24,0},{28,4},{1,9},{5... | collective-permute-start | bytes 589832 | tf_op jit(solution)/shard_map/ppermute | solution.py:55
  195.8 18.7 %collective-permute-start.101 = (bf16[128,768]{1,0:T(8,128)(2,1)S(1)}, bf16[128,768]{1,0:T(8,128)(2,1)S(1)}, u32[]{:S(2)}, u32[]{:S(2)}) collective-permute-start(bf16[128,768]{1,0:T(8,128)(2,1)S(1)} %collective-permute-done.100), channel_id=1, source_target_pairs={{0,8},{4,12},{8,16},{12,20},{16,24},{20,28},{24,0},{28,4},{1,9},{5... | collective-permute-start | bytes 589832 | tf_op jit(solution)/shard_map/ppermute | solution.py:55
  201.8 19.7 %collective-permute-start.11 = (bf16[128,1280]{1,0:T(8,128)(2,1)S(1)}, bf16[128,1280]{1,0:T(8,128)(2,1)S(1)}, u32[]{:S(2)}, u32[]{:S(2)}) collective-permute-start(bf16[128,1280]{1,0:T(8,128)(2,1)S(1)} %add_convert_fusion.23), channel_id=1, source_target_pairs={{0,8},{4,12},{8,16},{12,20},{16,24},{20,28},{24,0},{28,4},{1,9},{5... | collective-permute-start | bytes 983048 | tf_op jit(solution)/shard_map/ppermute | solution.py:44
  206.0 22.5 %collective-permute-start.60 = (bf16[128,1280]{1,0:T(8,128)(2,1)S(1)}, bf16[128,1280]{1,0:T(8,128)(2,1)S(1)}, u32[]{:S(2)}, u32[]{:S(2)}) collective-permute-start(bf16[128,1280]{1,0:T(8,128)(2,1)S(1)} %add_convert_fusion.19), channel_id=1, source_target_pairs={{0,8},{4,12},{8,16},{12,20},{16,24},{20,28},{24,0},{28,4},{1,9},{5... | collective-permute-start | bytes 983048 | tf_op jit(solution)/shard_map/ppermute | solution.py:44
  210.3 25.3 %collective-permute-start.103 = (bf16[128,1280]{1,0:T(8,128)(2,1)S(1)}, bf16[128,1280]{1,0:T(8,128)(2,1)S(1)}, u32[]{:S(2)}, u32[]{:S(2)}) collective-permute-start(bf16[128,1280]{1,0:T(8,128)(2,1)S(1)} %add_convert_fusion.15), channel_id=1, source_target_pairs={{0,8},{4,12},{8,16},{12,20},{16,24},{20,28},{24,0},{28,4},{1,9},{5... | collective-permute-start | bytes 983048 | tf_op jit(solution)/shard_map/ppermute | solution.py:44
  221.9 20.7 %collective-permute-start.12 = (bf16[128,1280]{1,0:T(8,128)(2,1)S(1)}, bf16[128,1280]{1,0:T(8,128)(2,1)S(1)}, u32[]{:S(2)}, u32[]{:S(2)}) collective-permute-start(bf16[128,1280]{1,0:T(8,128)(2,1)S(1)} %add_convert_fusion.22), channel_id=1, source_target_pairs={{0,8},{4,12},{8,16},{12,20},{16,24},{20,28},{24,0},{28,4},{1,9},{5... | collective-permute-start | bytes 983048 | tf_op jit(solution)/shard_map/ppermute | solution.py:44
  228.9 20.7 %collective-permute-start.61 = (bf16[128,1280]{1,0:T(8,128)(2,1)S(1)}, bf16[128,1280]{1,0:T(8,128)(2,1)S(1)}, u32[]{:S(2)}, u32[]{:S(2)}) collective-permute-start(bf16[128,1280]{1,0:T(8,128)(2,1)S(1)} %add_convert_fusion.18), channel_id=1, source_target_pairs={{0,8},{4,12},{8,16},{12,20},{16,24},{20,28},{24,0},{28,4},{1,9},{5... | collective-permute-start | bytes 983048 | tf_op jit(solution)/shard_map/ppermute | solution.py:44
  235.9 20.7 %collective-permute-start.104 = (bf16[128,1280]{1,0:T(8,128)(2,1)S(1)}, bf16[128,1280]{1,0:T(8,128)(2,1)S(1)}, u32[]{:S(2)}, u32[]{:S(2)}) collective-permute-start(bf16[128,1280]{1,0:T(8,128)(2,1)S(1)} %add_convert_fusion.14), channel_id=1, source_target_pairs={{0,8},{4,12},{8,16},{12,20},{16,24},{20,28},{24,0},{28,4},{1,9},{5... | collective-permute-start | bytes 983048 | tf_op jit(solution)/shard_map/ppermute | solution.py:44
  236.0 42.2 %collective-permute-start.17 = (bf16[640,512]{1,0:T(8,128)(2,1)S(1)}, bf16[640,512]{1,0:T(8,128)(2,1)S(1)}, u32[]{:S(2)}, u32[]{:S(2)}) collective-permute-start(bf16[640,512]{1,0:T(8,128)(2,1)S(1)} %copy-done.22), channel_id=1, source_target_pairs={{0,4},{4,0},{8,12},{12,8},{16,20},{20,16},{24,28},{28,24},{1,5},{5... | collective-permute-start | bytes 1966088 | tf_op jit(solution)/shard_map/ppermute | solution.py:33
  243.1 17.0 %collective-permute-start.13 = (bf16[128,640]{1,0:T(8,128)(2,1)S(1)}, bf16[128,640]{1,0:T(8,128)(2,1)S(1)}, u32[]{:S(2)}, u32[]{:S(2)}) collective-permute-start(bf16[128,640]{1,0:T(8,128)(2,1)S(1)} %get-tuple-element.85), channel_id=1, source_target_pairs={{0,8},{4,12},{8,16},{12,20},{16,24},{20,28},{24,0},{28,4},{1,9},{5... | collective-permute-start | bytes 491528 | tf_op jit(solution)/shard_map/ppermute | solution.py:55
  278.2 80.0 %collective-permute-start.27 = (bf16[512,1536]{1,0:T(8,128)(2,1)}, bf16[512,1536]{1,0:T(8,128)(2,1)S(1)}, u32[]{:S(2)}, u32[]{:S(2)}) collective-permute-start(bf16[512,1536]{1,0:T(8,128)(2,1)} %pad_maximum_fusion.3), channel_id=1, source_target_pairs={{0,4},{4,0},{8,12},{12,8},{16,20},{20,16},{24,28},{28,24},{1,5},{5... | collective-permute-start | bytes 4718600 | tf_op jit(solution)/shard_map/ppermute | solution.py:33
  293.4 16.9 %collective-permute-start.109 = (bf16[128,1024]{0,1:T(8,128)(2,1)S(1)}, bf16[128,1024]{0,1:T(8,128)(2,1)S(1)}, u32[]{:S(2)}, u32[]{:S(2)}) collective-permute-start(bf16[128,1024]{0,1:T(8,128)(2,1)S(1)} %dynamic-slice_convert_fusion.1), channel_id=1, source_target_pairs={{0,2},{1,3},{2,0},{3,1},{4,6},{5,7},{6,4},{7,5},{8,10},{9,11},{10,... | collective-permute-start | bytes 786440 | tf_op jit(solution)/shard_map/ppermute | solution.py:44
  300.2 17.5 %collective-permute-start.20 = (bf16[128,512]{0,1:T(8,128)(2,1)S(1)}, bf16[128,512]{0,1:T(8,128)(2,1)S(1)}, u32[]{:S(2)}, u32[]{:S(2)}) collective-permute-start(bf16[128,512]{0,1:T(8,128)(2,1)S(1)} %slice.435), channel_id=1, source_target_pairs={{0,4},{4,0},{8,12},{12,8},{16,20},{20,16},{24,28},{28,24},{1,5},{5... | collective-permute-start | bytes 393224 | tf_op jit(solution)/shard_map/ppermute | solution.py:33
  358.2 68.9 %collective-permute-start.34 = (bf16[512,1280]{1,0:T(8,128)(2,1)S(1)}, bf16[512,1280]{1,0:T(8,128)(2,1)S(1)}, u32[]{:S(2)}, u32[]{:S(2)}) collective-permute-start(bf16[512,1280]{1,0:T(8,128)(2,1)S(1)} %pad_maximum_fusion.7), channel_id=1, source_target_pairs={{0,4},{4,0},{8,12},{12,8},{16,20},{20,16},{24,28},{28,24},{1,5},{5... | collective-permute-start | bytes 3932168 | tf_op jit(solution)/shard_map/ppermute | solution.py:33
  370.7 13.8 %collective-permute-start.117 = (bf16[128,1536]{1,0:T(8,128)(2,1)S(1)}, bf16[128,1536]{1,0:T(8,128)(2,1)S(1)}, u32[]{:S(2)}, u32[]{:S(2)}) collective-permute-start(bf16[128,1536]{1,0:T(8,128)(2,1)S(1)} %fusion.5), channel_id=1, source_target_pairs={{0,8},{4,12},{8,16},{12,20},{16,24},{20,28},{24,0},{28,4},{1,9},{5... | collective-permute-start | bytes 1179656 | tf_op jit(solution)/shard_map/ppermute | solution.py:44
  372.3 20.7 %collective-permute-start.74 = (bf16[128,1536]{1,0:T(8,128)(2,1)S(1)}, bf16[128,1536]{1,0:T(8,128)(2,1)S(1)}, u32[]{:S(2)}, u32[]{:S(2)}) collective-permute-start(bf16[128,1536]{1,0:T(8,128)(2,1)S(1)} %fusion.3), channel_id=1, source_target_pairs={{0,8},{4,12},{8,16},{12,20},{16,24},{20,28},{24,0},{28,4},{1,9},{5... | collective-permute-start | bytes 1179656 | tf_op jit(solution)/shard_map/ppermute | solution.py:44
  374.2 27.2 %collective-permute-start.28 = (bf16[128,1536]{1,0:T(8,128)(2,1)S(1)}, bf16[128,1536]{1,0:T(8,128)(2,1)S(1)}, u32[]{:S(2)}, u32[]{:S(2)}) collective-permute-start(bf16[128,1536]{1,0:T(8,128)(2,1)S(1)} %fusion.1), channel_id=1, source_target_pairs={{0,8},{4,12},{8,16},{12,20},{16,24},{20,28},{24,0},{28,4},{1,9},{5... | collective-permute-start | bytes 1179656 | tf_op jit(solution)/shard_map/ppermute | solution.py:44
  385.0 24.9 %collective-permute-start.118 = (bf16[128,1536]{1,0:T(8,128)(2,1)S(1)}, bf16[128,1536]{1,0:T(8,128)(2,1)S(1)}, u32[]{:S(2)}, u32[]{:S(2)}) collective-permute-start(bf16[128,1536]{1,0:T(8,128)(2,1)S(1)} %add_convert_fusion.1), channel_id=1, source_target_pairs={{0,8},{4,12},{8,16},{12,20},{16,24},{20,28},{24,0},{28,4},{1,9},{5... | collective-permute-start | bytes 1179656 | tf_op jit(solution)/shard_map/ppermute | solution.py:44
  393.4 24.9 %collective-permute-start.75 = (bf16[128,1536]{1,0:T(8,128)(2,1)S(1)}, bf16[128,1536]{1,0:T(8,128)(2,1)S(1)}, u32[]{:S(2)}, u32[]{:S(2)}) collective-permute-start(bf16[128,1536]{1,0:T(8,128)(2,1)S(1)} %add_convert_fusion.5), channel_id=1, source_target_pairs={{0,8},{4,12},{8,16},{12,20},{16,24},{20,28},{24,0},{28,4},{1,9},{5... | collective-permute-start | bytes 1179656 | tf_op jit(solution)/shard_map/ppermute | solution.py:44
  401.8 24.9 %collective-permute-start.29 = (bf16[128,1536]{1,0:T(8,128)(2,1)S(1)}, bf16[128,1536]{1,0:T(8,128)(2,1)S(1)}, u32[]{:S(2)}, u32[]{:S(2)}) collective-permute-start(bf16[128,1536]{1,0:T(8,128)(2,1)S(1)} %add_convert_fusion.9), channel_id=1, source_target_pairs={{0,8},{4,12},{8,16},{12,20},{16,24},{20,28},{24,0},{28,4},{1,9},{5... | collective-permute-start | bytes 1179656 | tf_op jit(solution)/shard_map/ppermute | solution.py:44
  410.2 24.9 %collective-permute-start.119 = (bf16[128,1536]{1,0:T(8,128)(2,1)S(1)}, bf16[128,1536]{1,0:T(8,128)(2,1)S(1)}, u32[]{:S(2)}, u32[]{:S(2)}) collective-permute-start(bf16[128,1536]{1,0:T(8,128)(2,1)S(1)} %add_convert_fusion), channel_id=1, source_target_pairs={{0,8},{4,12},{8,16},{12,20},{16,24},{20,28},{24,0},{28,4},{1,9},{5... | collective-permute-start | bytes 1179656 | tf_op jit(solution)/shard_map/ppermute | solution.py:44
  418.7 24.9 %collective-permute-start.76 = (bf16[128,1536]{1,0:T(8,128)(2,1)S(1)}, bf16[128,1536]{1,0:T(8,128)(2,1)S(1)}, u32[]{:S(2)}, u32[]{:S(2)}) collective-permute-start(bf16[128,1536]{1,0:T(8,128)(2,1)S(1)} %add_convert_fusion.4), channel_id=1, source_target_pairs={{0,8},{4,12},{8,16},{12,20},{16,24},{20,28},{24,0},{28,4},{1,9},{5... | collective-permute-start | bytes 1179656 | tf_op jit(solution)/shard_map/ppermute | solution.py:44
  427.1 24.9 %collective-permute-start.30 = (bf16[128,1536]{1,0:T(8,128)(2,1)S(1)}, bf16[128,1536]{1,0:T(8,128)(2,1)S(1)}, u32[]{:S(2)}, u32[]{:S(2)}) collective-permute-start(bf16[128,1536]{1,0:T(8,128)(2,1)S(1)} %add_convert_fusion.8), channel_id=1, source_target_pairs={{0,8},{4,12},{8,16},{12,20},{16,24},{20,28},{24,0},{28,4},{1,9},{5... | collective-permute-start | bytes 1179656 | tf_op jit(solution)/shard_map/ppermute | solution.py:44
  427.6 31.4 %collective-permute-start.123 = (bf16[128,1280]{1,0:T(8,128)(2,1)S(1)}, bf16[128,1280]{1,0:T(8,128)(2,1)S(1)}, u32[]{:S(2)}, u32[]{:S(2)}) collective-permute-start(bf16[128,1280]{1,0:T(8,128)(2,1)S(1)} %fusion.11), channel_id=1, source_target_pairs={{0,8},{4,12},{8,16},{12,20},{16,24},{20,28},{24,0},{28,4},{1,9},{5... | collective-permute-start | bytes 983048 | tf_op jit(solution)/shard_map/ppermute | solution.py:44
  428.4 104.5 %collective-permute-start.41 = (bf16[768,512]{1,0:T(8,128)(2,1)S(1)}, bf16[768,512]{1,0:T(8,128)(2,1)S(1)}, u32[]{:S(2)}, u32[]{:S(2)}) collective-permute-start(bf16[768,512]{1,0:T(8,128)(2,1)S(1)} %copy-done.17), channel_id=1, source_target_pairs={{0,4},{4,0},{8,12},{12,8},{16,20},{20,16},{24,28},{28,24},{1,5},{5... | collective-permute-start | bytes 2359304 | tf_op jit(solution)/shard_map/ppermute | solution.py:33
  435.1 30.9 %collective-permute-start.80 = (bf16[128,1280]{1,0:T(8,128)(2,1)S(1)}, bf16[128,1280]{1,0:T(8,128)(2,1)S(1)}, u32[]{:S(2)}, u32[]{:S(2)}) collective-permute-start(bf16[128,1280]{1,0:T(8,128)(2,1)S(1)} %fusion.9), channel_id=1, source_target_pairs={{0,8},{4,12},{8,16},{12,20},{16,24},{20,28},{24,0},{28,4},{1,9},{5... | collective-permute-start | bytes 983048 | tf_op jit(solution)/shard_map/ppermute | solution.py:44
  443.5 29.5 %collective-permute-start.35 = (bf16[128,1280]{1,0:T(8,128)(2,1)S(1)}, bf16[128,1280]{1,0:T(8,128)(2,1)S(1)}, u32[]{:S(2)}, u32[]{:S(2)}) collective-permute-start(bf16[128,1280]{1,0:T(8,128)(2,1)S(1)} %fusion.7), channel_id=1, source_target_pairs={{0,8},{4,12},{8,16},{12,20},{16,24},{20,28},{24,0},{28,4},{1,9},{5... | collective-permute-start | bytes 983048 | tf_op jit(solution)/shard_map/ppermute | solution.py:44
  451.9 25.3 %collective-permute-start.120 = (bf16[128,768]{1,0:T(8,128)(2,1)S(1)}, bf16[128,768]{1,0:T(8,128)(2,1)S(1)}, u32[]{:S(2)}, u32[]{:S(2)}) collective-permute-start(bf16[128,768]{1,0:T(8,128)(2,1)S(1)} %get-tuple-element.55), channel_id=1, source_target_pairs={{0,8},{4,12},{8,16},{12,20},{16,24},{20,28},{24,0},{28,4},{1,9},{5... | collective-permute-start | bytes 589832 | tf_op jit(solution)/shard_map/ppermute | solution.py:55
  459.0 22.5 %collective-permute-start.77 = (bf16[128,768]{1,0:T(8,128)(2,1)S(1)}, bf16[128,768]{1,0:T(8,128)(2,1)S(1)}, u32[]{:S(2)}, u32[]{:S(2)}) collective-permute-start(bf16[128,768]{1,0:T(8,128)(2,1)S(1)} %get-tuple-element.67), channel_id=1, source_target_pairs={{0,8},{4,12},{8,16},{12,20},{16,24},{20,28},{24,0},{28,4},{1,9},{5... | collective-permute-start | bytes 589832 | tf_op jit(solution)/shard_map/ppermute | solution.py:55
  466.0 19.7 %collective-permute-start.31 = (bf16[128,768]{1,0:T(8,128)(2,1)S(1)}, bf16[128,768]{1,0:T(8,128)(2,1)S(1)}, u32[]{:S(2)}, u32[]{:S(2)}) collective-permute-start(bf16[128,768]{1,0:T(8,128)(2,1)S(1)} %get-tuple-element.79), channel_id=1, source_target_pairs={{0,8},{4,12},{8,16},{12,20},{16,24},{20,28},{24,0},{28,4},{1,9},{5... | collective-permute-start | bytes 589832 | tf_op jit(solution)/shard_map/ppermute | solution.py:55
  473.0 39.1 %collective-permute-start.124 = (bf16[128,1280]{1,0:T(8,128)(2,1)S(1)}, bf16[128,1280]{1,0:T(8,128)(2,1)S(1)}, u32[]{:S(2)}, u32[]{:S(2)}) collective-permute-start(bf16[128,1280]{1,0:T(8,128)(2,1)S(1)} %add_convert_fusion.13), channel_id=1, source_target_pairs={{0,8},{4,12},{8,16},{12,20},{16,24},{20,28},{24,0},{28,4},{1,9},{5... | collective-permute-start | bytes 983048 | tf_op jit(solution)/shard_map/ppermute | solution.py:44
  477.2 36.4 %collective-permute-start.81 = (bf16[128,1280]{1,0:T(8,128)(2,1)S(1)}, bf16[128,1280]{1,0:T(8,128)(2,1)S(1)}, u32[]{:S(2)}, u32[]{:S(2)}) collective-permute-start(bf16[128,1280]{1,0:T(8,128)(2,1)S(1)} %add_convert_fusion.17), channel_id=1, source_target_pairs={{0,8},{4,12},{8,16},{12,20},{16,24},{20,28},{24,0},{28,4},{1,9},{5... | collective-permute-start | bytes 983048 | tf_op jit(solution)/shard_map/ppermute | solution.py:44
  481.4 22.5 %collective-permute-start.121 = (bf16[128,768]{1,0:T(8,128)(2,1)S(1)}, bf16[128,768]{1,0:T(8,128)(2,1)S(1)}, u32[]{:S(2)}, u32[]{:S(2)}) collective-permute-start(bf16[128,768]{1,0:T(8,128)(2,1)S(1)} %collective-permute-done.120), channel_id=1, source_target_pairs={{0,8},{4,12},{8,16},{12,20},{16,24},{20,28},{24,0},{28,4},{1,9},{5... | collective-permute-start | bytes 589832 | tf_op jit(solution)/shard_map/ppermute | solution.py:55
  485.7 22.2 %collective-permute-start.78 = (bf16[128,768]{1,0:T(8,128)(2,1)S(1)}, bf16[128,768]{1,0:T(8,128)(2,1)S(1)}, u32[]{:S(2)}, u32[]{:S(2)}) collective-permute-start(bf16[128,768]{1,0:T(8,128)(2,1)S(1)} %collective-permute-done.77), channel_id=1, source_target_pairs={{0,8},{4,12},{8,16},{12,20},{16,24},{20,28},{24,0},{28,4},{1,9},{5... | collective-permute-start | bytes 589832 | tf_op jit(solution)/shard_map/ppermute | solution.py:55
  512.1 16.6 %collective-permute-start.79 = (bf16[128,768]{1,0:T(8,128)(2,1)S(1)}, bf16[128,768]{1,0:T(8,128)(2,1)S(1)}, u32[]{:S(2)}, u32[]{:S(2)}) collective-permute-start(bf16[128,768]{1,0:T(8,128)(2,1)S(1)} %collective-permute-done.78), channel_id=1, source_target_pairs={{0,8},{4,12},{8,16},{12,20},{16,24},{20,28},{24,0},{28,4},{1,9},{5... | collective-permute-start | bytes 589832 | tf_op jit(solution)/shard_map/ppermute | solution.py:55
  513.6 19.2 %collective-permute-start.33 = (bf16[128,768]{1,0:T(8,128)(2,1)S(1)}, bf16[128,768]{1,0:T(8,128)(2,1)S(1)}, u32[]{:S(2)}, u32[]{:S(2)}) collective-permute-start(bf16[128,768]{1,0:T(8,128)(2,1)S(1)} %collective-permute-done.32), channel_id=1, source_target_pairs={{0,8},{4,12},{8,16},{12,20},{16,24},{20,28},{24,0},{28,4},{1,9},{5... | collective-permute-start | bytes 589832 | tf_op jit(solution)/shard_map/ppermute | solution.py:55
  520.2 19.7 %collective-permute-start.125 = (bf16[128,1280]{1,0:T(8,128)(2,1)S(1)}, bf16[128,1280]{1,0:T(8,128)(2,1)S(1)}, u32[]{:S(2)}, u32[]{:S(2)}) collective-permute-start(bf16[128,1280]{1,0:T(8,128)(2,1)S(1)} %add_convert_fusion.12), channel_id=1, source_target_pairs={{0,8},{4,12},{8,16},{12,20},{16,24},{20,28},{24,0},{28,4},{1,9},{5... | collective-permute-start | bytes 983048 | tf_op jit(solution)/shard_map/ppermute | solution.py:44
  524.4 22.5 %collective-permute-start.82 = (bf16[128,1280]{1,0:T(8,128)(2,1)S(1)}, bf16[128,1280]{1,0:T(8,128)(2,1)S(1)}, u32[]{:S(2)}, u32[]{:S(2)}) collective-permute-start(bf16[128,1280]{1,0:T(8,128)(2,1)S(1)} %add_convert_fusion.16), channel_id=1, source_target_pairs={{0,8},{4,12},{8,16},{12,20},{16,24},{20,28},{24,0},{28,4},{1,9},{5... | collective-permute-start | bytes 983048 | tf_op jit(solution)/shard_map/ppermute | solution.py:44
  528.6 25.3 %collective-permute-start.37 = (bf16[128,1280]{1,0:T(8,128)(2,1)S(1)}, bf16[128,1280]{1,0:T(8,128)(2,1)S(1)}, u32[]{:S(2)}, u32[]{:S(2)}) collective-permute-start(bf16[128,1280]{1,0:T(8,128)(2,1)S(1)} %add_convert_fusion.20), channel_id=1, source_target_pairs={{0,8},{4,12},{8,16},{12,20},{16,24},{20,28},{24,0},{28,4},{1,9},{5... | collective-permute-start | bytes 983048 | tf_op jit(solution)/shard_map/ppermute | solution.py:44
  532.9 46.3 %collective-permute-start.42 = (bf16[640,512]{1,0:T(8,128)(2,1)S(1)}, bf16[640,512]{1,0:T(8,128)(2,1)S(1)}, u32[]{:S(2)}, u32[]{:S(2)}) collective-permute-start(bf16[640,512]{1,0:T(8,128)(2,1)S(1)} %copy-done.21), channel_id=1, source_target_pairs={{0,4},{4,0},{8,12},{12,8},{16,20},{20,16},{24,28},{28,24},{1,5},{5... | collective-permute-start | bytes 1966088 | tf_op jit(solution)/shard_map/ppermute | solution.py:33
  540.4 17.0 %collective-permute-start.126 = (bf16[128,640]{1,0:T(8,128)(2,1)S(1)}, bf16[128,640]{1,0:T(8,128)(2,1)S(1)}, u32[]{:S(2)}, u32[]{:S(2)}) collective-permute-start(bf16[128,640]{1,0:T(8,128)(2,1)S(1)} %get-tuple-element.57), channel_id=1, source_target_pairs={{0,8},{4,12},{8,16},{12,20},{16,24},{20,28},{24,0},{28,4},{1,9},{5... | collective-permute-start | bytes 491528 | tf_op jit(solution)/shard_map/ppermute | solution.py:55
  547.5 13.5 %collective-permute-start.83 = (bf16[128,640]{1,0:T(8,128)(2,1)S(1)}, bf16[128,640]{1,0:T(8,128)(2,1)S(1)}, u32[]{:S(2)}, u32[]{:S(2)}) collective-permute-start(bf16[128,640]{1,0:T(8,128)(2,1)S(1)} %get-tuple-element.69), channel_id=1, source_target_pairs={{0,8},{4,12},{8,16},{12,20},{16,24},{20,28},{24,0},{28,4},{1,9},{5... | collective-permute-start | bytes 491528 | tf_op jit(solution)/shard_map/ppermute | solution.py:55
  590.7 17.0 %collective-permute-start.44 = (bf16[128,1024]{0,1:T(8,128)(2,1)S(1)}, bf16[128,1024]{0,1:T(8,128)(2,1)S(1)}, u32[]{:S(2)}, u32[]{:S(2)}) collective-permute-start(bf16[128,1024]{0,1:T(8,128)(2,1)S(1)} %dynamic-slice_convert_fusion.4), channel_id=1, source_target_pairs={{0,2},{1,3},{2,0},{3,1},{4,6},{5,7},{6,4},{7,5},{8,10},{9,11},{10,... | collective-permute-start | bytes 786440 | tf_op jit(solution)/shard_map/ppermute | solution.py:44
  (112 other events, 925.5 us)
